TPU v7x, 512 devices: a whole 4x4x16 slice. The times are simulated.
512 devices in a mesh: rep: 2 (over z_hi), fs: 32 (over z_lo, y), tp: 8 (over x, core).
Axes of the slice: x: 4, y: 4, z: 16 (z_hi: 2, z_lo: 8; z = z_hi * 8 + z_lo), core: 2. Of those that a mesh axis runs over, the one named last changes fastest.
Arguments:
- tokens: bfloat16 [32768, 2048], P(('rep', 'fs')), may hold values from -6 to 6
- recurrence_branch_weight: bfloat16 [2048, 2048], P('fs', 'tp'), may hold values from -0.125 to 0.125
- gate_branch_weight: bfloat16 [2048, 2048], P('fs', 'tp'), may hold values from -0.125 to 0.125
- convolution_kernel: bfloat16 [4, 2048], P(None, 'tp'), may hold values from -3 to 3
- recurrence_gate_blockwise: bfloat16 [8, 256, 256], P('tp'), may hold values from -0.375 to 0.375
- input_gate_blockwise: bfloat16 [8, 256, 256], P('tp'), may hold values from -0.375 to 0.375
- channel_decay_param: float32 [2048], P('tp')
- token_decay_shift: float32 [32768, 2048], P(('rep', 'fs'), 'tp'), may hold values from -1 to 0
- recurrence_output_weight: bfloat16 [2048, 2048], P('tp', 'fs'), may hold values from -0.5 to 0.5
- first_norm_gain: float32 [2048], replicated, may hold values from 0.1 to 1.9
- feedforward_gate_weight: bfloat16 [2048, 5120], P('fs', 'tp'), may hold values from -0.125 to 0.125
- feedforward_up_weight: bfloat16 [2048, 5120], P('fs', 'tp'), may hold values from -0.125 to 0.125
- feedforward_down_weight: bfloat16 [5120, 2048], P('tp', 'fs'), may hold values from -0.15625 to 0.15625
- second_norm_gain: float32 [2048], replicated, may hold values from 0.1 to 1.9
Outputs:
- layer_out: bfloat16 [32768, 2048], P(('rep', 'fs', 'tp'))
All inputs are finite; a program needn't handle non-finite values.
Results may differ from a plain program's by a relative error of at most 0.02.
Values may be sent and summed in bfloat16 or wider, within the bound.
No kernel may reach another device: no remote copies, remote signals or barrier semaphores. Data moves between devices by JAX's collectives and lax.ppermute only.
A program may use at most 64 MiB of HBM per device.

v0:
```python
import jax
import jax.numpy as jnp
from jax import lax
from jax.experimental import pallas as pl
from jax.experimental.pallas import tpu as pltpu
from jax.sharding import Mesh
from jax.sharding import PartitionSpec as P

residual_scale = 1.4142135623730951
f32 = jnp.float32
bf16 = jnp.bfloat16
AROUND = ("r", "zh", "zl")
ANY = pl.BlockSpec(memory_space=pl.ANY)
HBM = pl.BlockSpec(memory_space=pltpu.HBM)
VMEM = pl.BlockSpec(memory_space=pltpu.VMEM)
SMEM = pl.BlockSpec(memory_space=pltpu.SMEM)


def copy_for_each(value, axis):
    copies = jnp.broadcast_to(value, (lax.axis_size(axis), *value.shape))
    return lax.all_to_all(copies, axis, split_axis=0, concat_axis=0, tiled=True)


def start_all(copies):
    for copy in copies:
        copy.start()


def wait_all(copies):
    for copy in copies:
        copy.wait()


def mix_kernel(
    tokens_hbm, weight_hbm, taps_ref, rec_ref, inp_ref, decay_ref, shift_hbm,
    branch_ref, tokens_ref, weight_ref, shift_ref, a_ref, b_ref, sems,
):
    first = [
        pltpu.make_async_copy(
            weight_hbm.at[y, :, zh], weight_ref.at[zh, :, y], sems.at[4 * zh + y]
        )
        for zh in range(2)
        for y in range(4)
    ]
    first.append(pltpu.make_async_copy(tokens_hbm, tokens_ref, sems.at[8]))
    late = pltpu.make_async_copy(shift_hbm, shift_ref, sems.at[9])
    start_all(first)
    late.start()
    wait_all(first)
    length, width = shift_ref.shape
    weight = weight_ref[...].reshape(-1, 2 * width)
    acc = jnp.dot(tokens_ref[...], weight, preferred_element_type=f32).astype(bf16).astype(f32)
    value = acc[:, :width]
    taps = taps_ref[...].astype(f32)
    count = taps.shape[0]
    row = lax.broadcasted_iota(jnp.int32, (length, width), 0)
    conv = value * taps[count - 1 : count, :]
    for back in range(1, count):
        moved = jnp.where(row >= back, pltpu.roll(value, back, 0), 0.0)
        conv = conv + moved * taps[count - 1 - back : count - back, :]
    conv = conv.astype(bf16)
    rate = jax.nn.sigmoid(jnp.dot(conv, rec_ref[...], preferred_element_type=f32))
    inlet = jax.nn.sigmoid(jnp.dot(conv, inp_ref[...], preferred_element_type=f32))
    param = decay_ref[...]
    softplus = jnp.maximum(-param, 0.0) + jnp.log1p(jnp.exp(-jnp.abs(param)))
    late.wait()
    log_a = rate * (-8.0 * softplus) + shift_ref[...]
    a = jnp.exp(log_a)
    drive = jnp.sqrt(-jnp.tanh(log_a) * (1.0 + a * a)) * inlet * conv.astype(f32)
    tiles = length // 8
    a = a.reshape(tiles, 8, width)
    b = drive.reshape(tiles, 8, width)
    sub = lax.broadcasted_iota(jnp.int32, (tiles, 8, width), 1)
    for step in (1, 2, 4):
        keep = sub >= step
        b = b + a * jnp.where(keep, pltpu.roll(b, step, 1), 0.0)
        a = a * jnp.where(keep, pltpu.roll(a, step, 1), 1.0)
    a_ref[...] = a
    b_ref[...] = b

    def body(tile, last):
        state = b_ref[tile] + a_ref[tile] * last
        b_ref[tile] = state
        return jnp.broadcast_to(state[7:8, :], (8, width))

    lax.fori_loop(0, tiles, body, jnp.zeros((8, width), f32), unroll=8)
    state = b_ref[...].reshape(length, width)
    branch_ref[...] = (state * jax.nn.gelu(acc[:, width:])).astype(bf16)


def mix(tokens, weight, taps, rec, inp, decay, shift):
    length, width = shift.shape
    return pl.pallas_call(
        mix_kernel,
        out_shape=jax.ShapeDtypeStruct((length, width), bf16),
        in_specs=[HBM, ANY, VMEM, VMEM, VMEM, VMEM, HBM],
        out_specs=VMEM,
        scratch_shapes=[
            pltpu.VMEM(tokens.shape, bf16),
            pltpu.VMEM((2, 4, 4, tokens.shape[1] // 32, 2 * width), bf16),
            pltpu.VMEM(shift.shape, f32),
            pltpu.VMEM((length // 8, 8, width), f32),
            pltpu.VMEM((length // 8, 8, width), f32),
            pltpu.SemaphoreType.DMA((10,)),
        ],
        name="mix",
        compiler_params=pltpu.CompilerParams(vmem_limit_bytes=16 << 20),
    )(tokens, weight, taps, rec, inp, decay.reshape(1, width), shift)


def last_dims(left, right):
    return lax.dot_general(left, right, (((1,), (1,)), ((), ())), preferred_element_type=f32)


def project_kernel(place_ref, branch_ref, weight_hbm, keep_ref, send_ref, weight_ref, sems):
    c = place_ref[0]
    copies = [
        pltpu.make_async_copy(
            weight_hbm.at[y, :, zh], weight_ref.at[zh, :, y], sems.at[4 * zh + y]
        )
        for zh in range(2)
        for y in range(4)
    ]
    start_all(copies)
    wait_all(copies)
    share = keep_ref.shape[1]
    weight = weight_ref[...].reshape(-1, branch_ref.shape[1])
    for out_ref, core in ((send_ref, 1 - c), (keep_ref, c)):
        rows = [
            branch_ref[pl.ds(pl.multiple_of((2 * x + core) * share, share), share), :]
            for x in range(keep_ref.shape[0])
        ]
        out = last_dims(jnp.concatenate(rows, axis=0), weight)
        out_ref[...] = out.astype(bf16).reshape(out_ref.shape)


def project(place, branch, weight, share):
    width = branch.shape[1]
    features = weight.size // width
    half = jax.ShapeDtypeStruct((branch.shape[0] // (2 * share), share, features), bf16)
    return pl.pallas_call(
        project_kernel,
        out_shape=(half, half),
        in_specs=[SMEM, VMEM, ANY],
        out_specs=(VMEM, VMEM),
        scratch_shapes=[
            pltpu.VMEM((2, 4, 4, features // 32, width), bf16),
            pltpu.SemaphoreType.DMA((8,)),
        ],
        name="project",
        compiler_params=pltpu.CompilerParams(vmem_limit_bytes=16 << 20),
    )(place, branch, weight)


def norm_rows(parts_hbm, residual_ref, gain_ref, parts_ref, sem):
    copy = pltpu.make_async_copy(parts_hbm, parts_ref, sem.at[0])
    copy.start()
    total = residual_scale * residual_ref[...].astype(f32)
    copy.wait()
    for x in range(parts_ref.shape[0]):
        total = total + parts_ref[x].astype(f32)
    center = total - jnp.mean(total, axis=-1, keepdims=True)
    variance = jnp.mean(center * center, axis=-1, keepdims=True)
    return (center * lax.rsqrt(variance + 1e-05) * gain_ref[...]).astype(bf16)


def norm_kernel(parts_hbm, residual_ref, gain_ref, out_ref, parts_ref, sem):
    out_ref[...] = norm_rows(parts_hbm, residual_ref, gain_ref, parts_ref, sem)


def copies_kernel(parts_hbm, residual_ref, gain_ref, out_ref, copies_ref, parts_ref, sem):
    out = norm_rows(parts_hbm, residual_ref, gain_ref, parts_ref, sem)
    out_ref[...] = out
    for x in range(copies_ref.shape[0]):
        copies_ref[x] = out


def norm(parts, residual, gain, copied):
    own = jax.ShapeDtypeStruct(residual.shape, bf16)
    copies = jax.ShapeDtypeStruct(parts.shape, bf16)
    return pl.pallas_call(
        copies_kernel if copied else norm_kernel,
        out_shape=(own, copies) if copied else own,
        in_specs=[ANY, VMEM, VMEM],
        out_specs=(VMEM, VMEM) if copied else VMEM,
        scratch_shapes=[pltpu.VMEM(parts.shape, bf16), pltpu.SemaphoreType.DMA((1,))],
        name="norm",
        compiler_params=pltpu.CompilerParams(vmem_limit_bytes=12 << 20),
    )(parts, residual, gain.reshape(1, -1))


def stage_kernel(place_ref, fed_hbm, gate_ref, up_ref, down_ref, sems):
    y = place_ref[1]
    height = gate_ref.shape[2]
    copies = []
    for at, away in enumerate((0, 3, 1, 2)):
        there = lax.rem(y + away, 4)
        for source, target in (
            (fed_hbm.at[0, :, at, :height], gate_ref.at[:, there]),
            (fed_hbm.at[1, :, at, :height], up_ref.at[:, there]),
            (fed_hbm.at[0, :, at, height:], down_ref.at[:, there, 0]),
            (fed_hbm.at[1, :, at, height:], down_ref.at[:, there, 1]),
        ):
            copies.append(pltpu.make_async_copy(source, target, sems.at[len(copies)]))
    start_all(copies)
    wait_all(copies)


def stage(place, fed):
    units = fed.shape[-1]
    height = fed.shape[3] * 2 // 3
    wide = jax.ShapeDtypeStruct((8, 4, height, units), bf16)
    down = jax.ShapeDtypeStruct((8, 4, 2, height // 2, units), bf16)
    return pl.pallas_call(
        stage_kernel,
        out_shape=(wide, wide, down),
        in_specs=[SMEM, HBM],
        out_specs=(VMEM, VMEM, VMEM),
        scratch_shapes=[pltpu.SemaphoreType.DMA((16,))],
        name="stage",
        compiler_params=pltpu.CompilerParams(vmem_limit_bytes=20 << 20),
    )(place, fed)


def feed_kernel(rows_hbm, gate_ref, up_ref, down_ref, out_ref, rows_ref, sem):
    copy = pltpu.make_async_copy(rows_hbm, rows_ref, sem.at[0])
    copy.start()
    copy.wait()
    units = gate_ref.shape[-1]
    rows = rows_ref[...].reshape(-1, rows_ref.shape[-1])
    gate = jnp.dot(rows, gate_ref[...].reshape(-1, units), preferred_element_type=f32)
    up = jnp.dot(rows, up_ref[...].reshape(-1, units), preferred_element_type=f32)
    hidden = (jax.nn.silu(gate) * up).astype(bf16)
    out = last_dims(hidden, down_ref[...].reshape(-1, units))
    out_ref[...] = out.astype(bf16).reshape(out_ref.shape)


def feed(rows, gate, up, down):
    return pl.pallas_call(
        feed_kernel,
        out_shape=jax.ShapeDtypeStruct(rows.shape, bf16),
        in_specs=[ANY, VMEM, VMEM, VMEM],
        out_specs=VMEM,
        scratch_shapes=[pltpu.VMEM(rows.shape, bf16), pltpu.SemaphoreType.DMA((1,))],
        name="feed",
        compiler_params=pltpu.CompilerParams(vmem_limit_bytes=16 << 20),
    )(rows, gate, up, down)


def to_partner(value):
    return lax.ppermute(value, "c", [(0, 1), (1, 0)])


def sideways(value, by):
    return lax.ppermute(value, "y", [(i, (i + by) % 4) for i in range(4)])


def sum_at_owner(keep, send):
    both = (keep.astype(f32) + to_partner(send).astype(f32)).astype(bf16)
    return lax.all_to_all(both, "x", 0, 0, tiled=True)


def local(
    tokens,
    recurrence_branch_weight,
    gate_branch_weight,
    convolution_kernel,
    recurrence_gate_blockwise,
    input_gate_blockwise,
    channel_decay_param,
    token_decay_shift,
    recurrence_output_weight,
    first_norm_gain,
    feedforward_gate_weight,
    feedforward_up_weight,
    feedforward_down_weight,
    second_norm_gain,
):
    length = tokens.shape[0]
    share = length // 8
    r = lax.axis_index("r")
    x, c = lax.axis_index("x"), lax.axis_index("c")
    place = jnp.stack([c, lax.axis_index("y")]).astype(jnp.int32)
    channels = recurrence_branch_weight.shape[1]

    down = feedforward_down_weight.T
    height = down.shape[0]
    fed = jnp.concatenate(
        [
            jnp.where(r == 0, feedforward_gate_weight, feedforward_up_weight),
            jnp.where(r == 0, down[: height // 2], down[height // 2 :]),
        ],
        axis=0,
    )
    moved = [sideways(fed, by) for by in (1, -1, 2)]
    fed_column = jnp.stack([fed, *moved])
    fed_all = lax.all_gather(fed_column, AROUND, axis=0, tiled=False)
    fed_all = fed_all.reshape(2, 8, 4, *fed.shape)

    first = jnp.concatenate(
        [recurrence_branch_weight, gate_branch_weight, recurrence_output_weight.T], axis=1
    )
    pair = copy_for_each(first, "zh")
    line = copy_for_each(pair, "zl")
    branch_weight = copy_for_each(line[..., : 2 * channels], "y")
    output_weight = copy_for_each(line[..., 2 * channels :], "y")

    branch = mix(
        tokens,
        branch_weight,
        convolution_kernel,
        recurrence_gate_blockwise[0],
        input_gate_blockwise[0],
        channel_decay_param,
        token_decay_shift,
    )
    mixed = sum_at_owner(*project(place, branch, output_weight, share))
    own_tokens = lax.dynamic_slice_in_dim(tokens, (2 * x + c) * share, share, 0)
    normed, copies = norm(mixed, own_tokens, first_norm_gain, True)
    mine = lax.all_to_all(copies, "x", 0, 0, tiled=True)
    other = to_partner(mine)
    staged = stage(place, fed_all)
    keep = feed(mine, *staged)
    ffn = sum_at_owner(keep, feed(other, *staged))
    return norm(ffn, normed, second_norm_gain, False)


def solution(mesh):
    fine = Mesh(mesh.devices.reshape(2, 2, 4, 4, 4, 2), ("r", "zh", "zl", "y", "x", "c"))
    fs = ("zh", "zl", "y")
    tp = ("x", "c")
    return jax.shard_map(
        local,
        mesh=fine,
        in_specs=(
            P(("r", *fs), None),
            P(fs, tp),
            P(fs, tp),
            P(None, tp),
            P(tp, None, None),
            P(tp, None, None),
            P(tp),
            P(("r", *fs), tp),
            P(tp, fs),
            P(),
            P(fs, tp),
            P(fs, tp),
            P(tp, fs),
            P(),
        ),
        out_specs=P(("r", *fs, *tp), None),
        check_vma=False,
    )
```

profile of v0, /device:TPU:288, one launch (start us, length us, event | category | flops | bytes accessed | tf_op | source)
XLA Modules:
  0.0 209.2 jit_solution(4482618470526734538)
XLA Ops:
  8.3 4.9 %collective-permute-start.2 = (bf16[96,640]{1,0:T(8,128)(2,1)S(1)}, bf16[96,640]{1,0:T(8,128)(2,1)S(1)}, u32[]{:S(2)}, u32[]{:S(2)}) collective-permute-start(bf16[96,640]{1,0:T(8,128)(2,1)S(1)} %get-tuple-element.20), channel_id=1, source_target_pairs={{0,24},{8,0},{16,8},{24,16},{1,25},{9,1},{17,9},{25,17},{2,26},{10... | collective-permute-start | bytes 368648 | tf_op jit(solution)/shard_map/ppermute | solution.py:255
  13.2 2.5 %collective-permute-start.3 = (bf16[96,640]{1,0:T(8,128)(2,1)S(1)}, bf16[96,640]{1,0:T(8,128)(2,1)S(1)}, u32[]{:S(2)}, u32[]{:S(2)}) collective-permute-start(bf16[96,640]{1,0:T(8,128)(2,1)S(1)} %get-tuple-element.20), channel_id=1, source_target_pairs={{0,16},{8,24},{16,0},{24,8},{1,17},{9,25},{17,1},{25,9},{2,18},{10... | collective-permute-start | bytes 368648 | tf_op jit(solution)/shard_map/ppermute | solution.py:255
  15.8 2.9 %collective-permute-start.1 = (bf16[96,640]{1,0:T(8,128)(2,1)S(1)}, bf16[96,640]{1,0:T(8,128)(2,1)S(1)}, u32[]{:S(2)}, u32[]{:S(2)}) collective-permute-start(bf16[96,640]{1,0:T(8,128)(2,1)S(1)} %get-tuple-element.20), channel_id=1, source_target_pairs={{0,8},{8,16},{16,24},{24,0},{1,9},{9,17},{17,25},{25,1},{2,10},{10... | collective-permute-start | bytes 368648 | tf_op jit(solution)/shard_map/ppermute | solution.py:255
  18.7 3.6 %collective-permute-done.3 = bf16[96,640]{1,0:T(8,128)(2,1)S(1)} collective-permute-done((bf16[96,640]{1,0:T(8,128)(2,1)S(1)}, bf16[96,640]{1,0:T(8,128)(2,1)S(1)}, u32[]{:S(2)}, u32[]{:S(2)}) %collective-permute-start.3) | collective-permute-done | bytes 122912 | tf_op jit(solution)/shard_map/ppermute | solution.py:255
  22.3 1.9 collective-permute-done.1
  25.1 15.5 %all_to_all.35 = bf16[2,64,768]{2,1,0:T(8,128)(2,1)S(1)} all-to-all(bf16[2,64,768]{2,1,0:T(8,128)(2,1)S(1)} %broadcast_in_dim.12), channel_id=1, replica_groups=mesh['r'=2,'zh'=2,'zl'=4,'y'=4,'x'=4,'c'=2] {'zh'}, dimensions={0} | all-to-all | bytes 393216 | tf_op jit(solution)/shard_map/all_to_all | solution.py:21
  40.7 34.5 %all_to_all.36 = bf16[4,2,64,768]{3,2,1,0:T(8,128)(2,1)S(1)} all-to-all(bf16[4,2,64,768]{3,2,1,0:T(8,128)(2,1)S(1)} %broadcast_in_dim.13), channel_id=1, replica_groups=mesh['r'=2,'zh'=2,'zl'=4,'y'=4,'x'=4,'c'=2] {'zl'}, dimensions={0} | all-to-all | bytes 1572864 | tf_op jit(solution)/shard_map/all_to_all | solution.py:21
  76.9 3.6 %all-to-all-start.2 = ((bf16[4,4,2,64,512]{4,3,2,1,0:T(8,128)(2,1)}), bf16[4,4,2,64,512]{4,3,2,1,0:T(8,128)(2,1)S(1)}, u32[]{:S(2)}, u32[]{:S(2)}) async-start(bf16[4,4,2,64,512]{4,3,2,1,0:T(8,128)(2,1)} %broadcast_in_dim.14), calls=%async_computation.2 | async-start | bytes 4194304 | tf_op jit(solution)/shard_map/all_to_all | solution.py:21
  80.6 25.1 %all-to-all-done.2.weight_hbm = bf16[4,4,2,64,512]{4,3,2,1,0:T(8,128)(2,1)S(1)} async-done(((bf16[4,4,2,64,512]{4,3,2,1,0:T(8,128)(2,1)}), bf16[4,4,2,64,512]{4,3,2,1,0:T(8,128)(2,1)S(1)}, u32[]{:S(2)}, u32[]{:S(2)}) %all-to-all-start.2) | async-done | bytes 2097184 | tf_op jit(solution)/shard_map/all_to_all | solution.py:21
  106.9 3.5 %all-to-all-start.3 = ((bf16[4,4,2,64,256]{4,3,2,1,0:T(8,128)(2,1)}), bf16[4,4,2,64,256]{4,3,2,1,0:T(8,128)(2,1)S(1)}, u32[]{:S(2)}, u32[]{:S(2)}) async-start(bf16[4,4,2,64,256]{4,3,2,1,0:T(8,128)(2,1)} %broadcast_in_dim.15), calls=%async_computation.3 | async-start | bytes 2097152 | tf_op jit(solution)/shard_map/all_to_all | solution.py:21
  114.0 3.2 %mix.1.branch_ref = bf16[512,256]{1,0:T(8,128)(2,1)S(1)} custom-call(bf16[512,2048]{1,0:T(8,128)(2,1)S(1)} %copy-done.1, bf16[4,4,2,64,512]{4,3,2,1,0:T(8,128)(2,1)S(1)} %all-to-all-done.2.weight_hbm, bf16[4,256]{1,0:T(4,128)(2,1)S(1)} %copy-done.7, bf16[256,256]{1,0:T(8,128)(2,1)S(1)} %bitcast.16, bf16[256,256]{1,0:T(8,128)(2,1)S(1)} %bitcast.17, ...), custom_call_target="tpu_custom_call" | custom-call | tf_op jit(solution)/shard_map/mix/pallas_call | solution.py:93
  117.2 6.2 %all-to-all-done.3.weight_hbm = bf16[4,4,2,64,256]{4,3,2,1,0:T(8,128)(2,1)S(1)} async-done(((bf16[4,4,2,64,256]{4,3,2,1,0:T(8,128)(2,1)}), bf16[4,4,2,64,256]{4,3,2,1,0:T(8,128)(2,1)S(1)}, u32[]{:S(2)}, u32[]{:S(2)}) %all-to-all-start.3) | async-done | bytes 1048608 | tf_op jit(solution)/shard_map/all_to_all | solution.py:21
  123.4 1.7 project.1
  125.2 1.9 collective-permute-start
  127.1 2.6 %collective-permute-done = bf16[4,64,2048]{2,1,0:T(8,128)(2,1)S(1)} collective-permute-done((bf16[4,64,2048]{2,1,0:T(8,128)(2,1)S(1)}, bf16[4,64,2048]{2,1,0:T(8,128)(2,1)S(1)}, u32[]{:S(2)}, u32[]{:S(2)}) %collective-permute-start) | collective-permute-done | bytes 1048608 | tf_op jit(solution)/shard_map/ppermute | solution.py:251
  131.2 4.3 %all-to-all-start.4 = ((bf16[4,64,2048]{2,1,0:T(8,128)(2,1)}), bf16[4,64,2048]{2,1,0:T(8,128)(2,1)S(1)}, u32[]{:S(2)}, u32[]{:S(2)}) async-start(bf16[4,64,2048]{2,1,0:T(8,128)(2,1)} %add_convert_fusion.1), calls=%async_computation.4 | async-start | bytes 2097152 | tf_op jit(solution)/shard_map/all_to_all | solution.py:260
  136.4 14.4 %all-to-all-done.4.parts_hbm = bf16[4,64,2048]{2,1,0:T(8,128)(2,1)S(1)} async-done(((bf16[4,64,2048]{2,1,0:T(8,128)(2,1)}), bf16[4,64,2048]{2,1,0:T(8,128)(2,1)S(1)}, u32[]{:S(2)}, u32[]{:S(2)}) %all-to-all-start.4) | async-done | bytes 1048608 | tf_op jit(solution)/shard_map/all_to_all | solution.py:260
  151.3 17.0 %all_to_all.37.rows_hbm = bf16[4,64,2048]{2,1,0:T(8,128)(2,1)S(1)} all-to-all(bf16[4,64,2048]{2,1,0:T(8,128)(2,1)S(1)} %get-tuple-element.14), channel_id=1, replica_groups=mesh['r'=2,'zh'=2,'zl'=4,'y'=4,'x'=4,'c'=2] {'x'}, dimensions={0} | all-to-all | bytes 2097152 | tf_op jit(solution)/shard_map/all_to_all | solution.py:320
  168.3 1.9 collective-permute-start.4
  170.2 3.2 %copy-done = bf16[64,96,640]{2,1,0:T(8,128)(2,1)S(1)} copy-done((bf16[64,96,640]{2,1,0:T(8,128)(2,1)S(1)}, bf16[64,96,640]{2,1,0:T(8,128)(2,1)}, u32[]{:S(2)}) %copy-start) | copy-done | bytes 7864344
  174.9 2.7 %feed.3 = bf16[4,64,2048]{2,1,0:T(8,128)(2,1)S(1)} custom-call(bf16[4,64,2048]{2,1,0:T(8,128)(2,1)S(1)} %collective-permute-done.4.rows_hbm, bf16[8,4,64,640]{3,2,1,0:T(8,128)(2,1)S(1)} %get-tuple-element.15.gate_ref, bf16[8,4,64,640]{3,2,1,0:T(8,128)(2,1)S(1)} %get-tuple-element.16.up_ref, bf16[8,4,2,32,640]{4,3,2,1,0:T(8,128)(2,1)S(1)} %get-tuple-element.17.down_ref), custom_call_target="tpu_custom_call" | custom-call | tf_op jit(solution)/shard_map/feed/pallas_call | solution.py:239
  177.6 2.4 %collective-permute-start.5 = (bf16[4,64,2048]{2,1,0:T(8,128)(2,1)S(1)}, bf16[4,64,2048]{2,1,0:T(8,128)(2,1)S(1)}, u32[]{:S(2)}, u32[]{:S(2)}) collective-permute-start(bf16[4,64,2048]{2,1,0:T(8,128)(2,1)S(1)} %feed.3), channel_id=1, source_target_pairs={{0,1},{1,0},{2,3},{3,2},{4,5},{5,4},{6,7},{7,6},{8,9},{9,8},{10,11... | collective-permute-start | bytes 3145736 | tf_op jit(solution)/shard_map/ppermute | solution.py:251
  180.0 2.7 %feed.2 = bf16[4,64,2048]{2,1,0:T(8,128)(2,1)S(1)} custom-call(bf16[4,64,2048]{2,1,0:T(8,128)(2,1)S(1)} %all_to_all.37.rows_hbm, bf16[8,4,64,640]{3,2,1,0:T(8,128)(2,1)S(1)} %get-tuple-element.15.gate_ref, bf16[8,4,64,640]{3,2,1,0:T(8,128)(2,1)S(1)} %get-tuple-element.16.up_ref, bf16[8,4,2,32,640]{4,3,2,1,0:T(8,128)(2,1)S(1)} %get-tuple-element.17.down_ref), custom_call_target="tpu_custom_call" | custom-call | tf_op jit(solution)/shard_map/feed/pallas_call | solution.py:239
  183.2 18.0 %all_to_all.38.parts_hbm = bf16[4,64,2048]{2,1,0:T(8,128)(2,1)S(1)} all-to-all(bf16[4,64,2048]{2,1,0:T(8,128)(2,1)S(1)} %add_convert_fusion), channel_id=1, replica_groups=mesh['r'=2,'zh'=2,'zl'=4,'y'=4,'x'=4,'c'=2] {'x'}, dimensions={0} | all-to-all | bytes 2097152 | tf_op jit(solution)/shard_map/all_to_all | solution.py:260
  (47 shorter events, 15.2 us)
Async XLA Ops:
  6.5 18.5 %copy-start.9 = (bf16[256,64]{0,1:T(8,128)(2,1)S(1)}, bf16[256,64]{0,1:T(8,128)(2,1)}, u32[]{:S(2)}) copy-start(bf16[256,64]{0,1:T(8,128)(2,1)} %param.22) | copy-start | bytes 98308
  6.5 18.6 %copy-start.11 = (bf16[64,256]{1,0:T(8,128)(2,1)S(1)}, bf16[64,256]{1,0:T(8,128)(2,1)}, u32[]{:S(2)}) copy-start(bf16[64,256]{1,0:T(8,128)(2,1)} %param.15) | copy-start | bytes 98308
  6.5 18.6 %copy-start.10 = (bf16[64,256]{1,0:T(8,128)(2,1)S(1)}, bf16[64,256]{1,0:T(8,128)(2,1)}, u32[]{:S(2)}) copy-start(bf16[64,256]{1,0:T(8,128)(2,1)} %param.16) | copy-start | bytes 98308
  6.5 163.7 %all-gather.3.cloned.1.call-start = ((), (), s32[]{:S(2)}) async-start(), calls=%async_computation.7 | async-start | bytes 8355840 | tf_op jit(solution)/shard_map/all_gather | solution.py:297
  8.3 10.4 %collective-permute-start.2 = (bf16[96,640]{1,0:T(8,128)(2,1)S(1)}, bf16[96,640]{1,0:T(8,128)(2,1)S(1)}, u32[]{:S(2)}, u32[]{:S(2)}) collective-permute-start(bf16[96,640]{1,0:T(8,128)(2,1)S(1)} %get-tuple-element.20), channel_id=1, source_target_pairs={{0,24},{8,0},{16,8},{24,16},{1,25},{9,1},{17,9},{25,17},{2,26},{10... | collective-permute-start | bytes 368648 | tf_op jit(solution)/shard_map/ppermute | solution.py:255
  13.2 9.1 %collective-permute-start.3 = (bf16[96,640]{1,0:T(8,128)(2,1)S(1)}, bf16[96,640]{1,0:T(8,128)(2,1)S(1)}, u32[]{:S(2)}, u32[]{:S(2)}) collective-permute-start(bf16[96,640]{1,0:T(8,128)(2,1)S(1)} %get-tuple-element.20), channel_id=1, source_target_pairs={{0,16},{8,24},{16,0},{24,8},{1,17},{9,25},{17,1},{25,9},{2,18},{10... | collective-permute-start | bytes 368648 | tf_op jit(solution)/shard_map/ppermute | solution.py:255
  15.8 8.4 %collective-permute-start.1 = (bf16[96,640]{1,0:T(8,128)(2,1)S(1)}, bf16[96,640]{1,0:T(8,128)(2,1)S(1)}, u32[]{:S(2)}, u32[]{:S(2)}) collective-permute-start(bf16[96,640]{1,0:T(8,128)(2,1)S(1)} %get-tuple-element.20), channel_id=1, source_target_pairs={{0,8},{8,16},{16,24},{24,0},{1,9},{9,17},{17,25},{25,1},{2,10},{10... | collective-permute-start | bytes 368648 | tf_op jit(solution)/shard_map/ppermute | solution.py:255
  76.9 28.8 %all-to-all-start.2 = ((bf16[4,4,2,64,512]{4,3,2,1,0:T(8,128)(2,1)}), bf16[4,4,2,64,512]{4,3,2,1,0:T(8,128)(2,1)S(1)}, u32[]{:S(2)}, u32[]{:S(2)}) async-start(bf16[4,4,2,64,512]{4,3,2,1,0:T(8,128)(2,1)} %broadcast_in_dim.14), calls=%async_computation.2 | async-start | bytes 4194304 | tf_op jit(solution)/shard_map/all_to_all | solution.py:21
  80.5 30.0 %copy-start.3 = (bf16[1,256,256]{2,1,0:T(8,128)(2,1)S(1)}, bf16[1,256,256]{2,1,0:T(8,128)(2,1)}, u32[]{:S(2)}) copy-start(bf16[1,256,256]{2,1,0:T(8,128)(2,1)} %param.18) | copy-start | bytes 393220
  80.5 29.9 %copy-start.7 = (bf16[4,256]{1,0:T(4,128)(2,1)S(1)}, bf16[4,256]{1,0:T(4,128)(2,1)}, u32[]{:S(2)}) copy-start(bf16[4,256]{1,0:T(4,128)(2,1)} %taps_ref.1) | copy-start | bytes 6148
  80.5 29.9 %copy-start.8 = (f32[256]{0:T(256)S(1)}, f32[256]{0:T(256)}, u32[]{:S(2)}) copy-start(f32[256]{0:T(256)} %param.20) | copy-start | bytes 3076
  106.9 16.6 %all-to-all-start.3 = ((bf16[4,4,2,64,256]{4,3,2,1,0:T(8,128)(2,1)}), bf16[4,4,2,64,256]{4,3,2,1,0:T(8,128)(2,1)S(1)}, u32[]{:S(2)}, u32[]{:S(2)}) async-start(bf16[4,4,2,64,256]{4,3,2,1,0:T(8,128)(2,1)} %broadcast_in_dim.15), calls=%async_computation.3 | async-start | bytes 2097152 | tf_op jit(solution)/shard_map/all_to_all | solution.py:21
  110.5 1.6 copy-start.1
  112.1 1.0 copy-start.2
  113.1 0.9 copy-start.4
  125.2 4.6 %collective-permute-start = (bf16[4,64,2048]{2,1,0:T(8,128)(2,1)S(1)}, bf16[4,64,2048]{2,1,0:T(8,128)(2,1)S(1)}, u32[]{:S(2)}, u32[]{:S(2)}) collective-permute-start(bf16[4,64,2048]{2,1,0:T(8,128)(2,1)S(1)} %get-tuple-element.13), channel_id=1, source_target_pairs={{0,1},{1,0},{2,3},{3,2},{4,5},{5,4},{6,7},{7,6},{8,9},{9,8},{10,11... | collective-permute-start | bytes 3145736 | tf_op jit(solution)/shard_map/ppermute | solution.py:251
  131.2 19.7 %copy-start.5 = (f32[2048]{0:T(1024)S(1)}, f32[2048]{0:T(1024)}, u32[]{:S(2)}) copy-start(f32[2048]{0:T(1024)} %param.23) | copy-start | bytes 24580
  131.2 19.7 %all-to-all-start.4 = ((bf16[4,64,2048]{2,1,0:T(8,128)(2,1)}), bf16[4,64,2048]{2,1,0:T(8,128)(2,1)S(1)}, u32[]{:S(2)}, u32[]{:S(2)}) async-start(bf16[4,64,2048]{2,1,0:T(8,128)(2,1)} %add_convert_fusion.1), calls=%async_computation.4 | async-start | bytes 2097152 | tf_op jit(solution)/shard_map/all_to_all | solution.py:260
  168.3 6.6 %collective-permute-start.4 = (bf16[4,64,2048]{2,1,0:T(8,128)(2,1)S(1)}, bf16[4,64,2048]{2,1,0:T(8,128)(2,1)S(1)}, u32[]{:S(2)}, u32[]{:S(2)}) collective-permute-start(bf16[4,64,2048]{2,1,0:T(8,128)(2,1)S(1)} %all_to_all.37.rows_hbm), channel_id=1, source_target_pairs={{0,1},{1,0},{2,3},{3,2},{4,5},{5,4},{6,7},{7,6},{8,9},{9,8},{10,11... | collective-permute-start | bytes 3145736 | tf_op jit(solution)/shard_map/ppermute | solution.py:251
  170.2 3.2 %copy-start = (bf16[64,96,640]{2,1,0:T(8,128)(2,1)S(1)}, bf16[64,96,640]{2,1,0:T(8,128)(2,1)}, u32[]{:S(2)}) copy-start(bf16[64,96,640]{2,1,0:T(8,128)(2,1)} %all-gather.3.cloned.1.call-done) | copy-start | bytes 23592964
  177.6 5.1 %collective-permute-start.5 = (bf16[4,64,2048]{2,1,0:T(8,128)(2,1)S(1)}, bf16[4,64,2048]{2,1,0:T(8,128)(2,1)S(1)}, u32[]{:S(2)}, u32[]{:S(2)}) collective-permute-start(bf16[4,64,2048]{2,1,0:T(8,128)(2,1)S(1)} %feed.3), channel_id=1, source_target_pairs={{0,1},{1,0},{2,3},{3,2},{4,5},{5,4},{6,7},{7,6},{8,9},{9,8},{10,11... | collective-permute-start | bytes 3145736 | tf_op jit(solution)/shard_map/ppermute | solution.py:251
  182.7 18.4 %copy-start.6 = (f32[2048]{0:T(1024)S(1)}, f32[2048]{0:T(1024)}, u32[]{:S(2)}) copy-start(f32[2048]{0:T(1024)} %param.27) | copy-start | bytes 24580
Sparse Core Ops, SparseCore 0:
  25.2 113.6 all-gather.2
where the time goes:
time: 210 us; the launch traced here: 209 us
  blocking collectives  84.9 us (40%)
  waiting for transfers between devices  53.9 us (26%)
  starting transfers between devices  28 us (13%)
  between operations  13.7 us (7%)
  Pallas kernels  13.4 us (6%)
  local copies, waits for them, and re-layouts  10.8 us (5%)
  other arithmetic  4.57 us (2%)
    all_to_all x2, blocking collectives, copy_for_each(): return lax.all_to_all(copies, axis, split_axis=0, concat_axis=0, tiled=True)  50 us
    all_to_all x2, waiting for transfers between devices, copy_for_each(): return lax.all_to_all(copies, axis, split_axis=0, concat_axis=0, tiled=True)  31.3 us
    all_to_all x1, blocking collectives, sum_at_owner(): return lax.all_to_all(both, 'x', 0, 0, tiled=True)  18 us
    all_to_all x1, blocking collectives, local(): mine = lax.all_to_all(copies, 'x', 0, 0, tiled=True)  17 us
    all_to_all x1, waiting for transfers between devices, sum_at_owner(): return lax.all_to_all(both, 'x', 0, 0, tiled=True)  14.4 us
    ppermute x3, starting transfers between devices, sideways(): return lax.ppermute(value, 'y', [(i, (i + by) % 4) for i in range(4)])  10.3 us
    all_to_all x2, starting transfers between devices, copy_for_each(): return lax.all_to_all(copies, axis, split_axis=0, concat_axis=0, tiled=True)  7.13 us
    unnamed x24, local copies, waits for them, and re-layouts  6.82 us
  transfers between devices with their start and end apart: 10, of which 6 were waited for; matrix products, arithmetic and copies ran while one was open for 3% of the time, Pallas kernels for 5%

commit v1 on v0

--- a/solution.py
+++ b/solution.py
@@ -31,19 +31,29 @@
         copy.wait()
 
 
-def mix_kernel(
-    tokens_hbm, weight_hbm, taps_ref, rec_ref, inp_ref, decay_ref, shift_hbm,
-    branch_ref, tokens_ref, weight_ref, shift_ref, a_ref, b_ref, sems,
-):
-    first = [
-        pltpu.make_async_copy(
-            weight_hbm.at[y, :, zh], weight_ref.at[zh, :, y], sems.at[4 * zh + y]
-        )
-        for zh in range(2)
-        for y in range(4)
-    ]
-    first.append(pltpu.make_async_copy(tokens_hbm, tokens_ref, sems.at[8]))
-    late = pltpu.make_async_copy(shift_hbm, shift_ref, sems.at[9])
+def loads(pieces, target, y, sems):
+    copies = []
+    half = target.shape[1] // 2
+    for away, piece, begin in zip((0, 3, 1, 2, 2), pieces, (0, 0, 0, 0, half)):
+        for zh in range(2):
+            rows = pl.ds(begin, piece.shape[0])
+            copies.append(
+                pltpu.make_async_copy(
+                    piece.at[:, zh],
+                    target.at[zh, rows, lax.rem(y + away, 4)],
+                    sems.at[len(copies)],
+                )
+            )
+    return copies
+
+
+def mix_kernel(place_ref, tokens_hbm, *refs):
+    pieces, refs = refs[:5], refs[5:]
+    taps_ref, rec_ref, inp_ref, decay_ref, shift_hbm, branch_ref = refs[:6]
+    tokens_ref, weight_ref, shift_ref, a_ref, b_ref, sems = refs[6:]
+    first = loads(pieces, weight_ref, place_ref[1], sems)
+    first.append(pltpu.make_async_copy(tokens_hbm, tokens_ref, sems.at[10]))
+    late = pltpu.make_async_copy(shift_hbm, shift_ref, sems.at[11])
     start_all(first)
     late.start()
     wait_all(first)
@@ -88,12 +98,12 @@
     branch_ref[...] = (state * jax.nn.gelu(acc[:, width:])).astype(bf16)
 
 
-def mix(tokens, weight, taps, rec, inp, decay, shift):
+def mix(place, tokens, pieces, taps, rec, inp, decay, shift):
     length, width = shift.shape
     return pl.pallas_call(
         mix_kernel,
         out_shape=jax.ShapeDtypeStruct((length, width), bf16),
-        in_specs=[HBM, ANY, VMEM, VMEM, VMEM, VMEM, HBM],
+        in_specs=[SMEM, HBM] + [ANY] * 5 + [VMEM] * 4 + [HBM],
         out_specs=VMEM,
         scratch_shapes=[
             pltpu.VMEM(tokens.shape, bf16),
@@ -101,55 +111,49 @@
             pltpu.VMEM(shift.shape, f32),
             pltpu.VMEM((length // 8, 8, width), f32),
             pltpu.VMEM((length // 8, 8, width), f32),
-            pltpu.SemaphoreType.DMA((10,)),
+            pltpu.SemaphoreType.DMA((12,)),
         ],
         name="mix",
-        compiler_params=pltpu.CompilerParams(vmem_limit_bytes=16 << 20),
-    )(tokens, weight, taps, rec, inp, decay.reshape(1, width), shift)
+        compiler_params=pltpu.CompilerParams(vmem_limit_bytes=60 << 20),
+    )(place, tokens, *pieces, taps, rec, inp, decay.reshape(1, width), shift)
 
 
 def last_dims(left, right):
     return lax.dot_general(left, right, (((1,), (1,)), ((), ())), preferred_element_type=f32)
 
 
-def project_kernel(place_ref, branch_ref, weight_hbm, keep_ref, send_ref, weight_ref, sems):
-    c = place_ref[0]
-    copies = [
-        pltpu.make_async_copy(
-            weight_hbm.at[y, :, zh], weight_ref.at[zh, :, y], sems.at[4 * zh + y]
-        )
-        for zh in range(2)
-        for y in range(4)
+def project_kernel(place_ref, branch_ref, *refs):
+    pieces, (out_ref, weight_ref, sems) = refs[:5], refs[5:]
+    core = place_ref[0]
+    copies = loads(pieces, weight_ref, place_ref[1], sems)
+    start_all(copies)
+    share = out_ref.shape[1]
+    rows = [
+        branch_ref[pl.ds(pl.multiple_of((2 * x + core) * share, share), share), :]
+        for x in range(out_ref.shape[0])
     ]
-    start_all(copies)
     wait_all(copies)
-    share = keep_ref.shape[1]
-    weight = weight_ref[...].reshape(-1, branch_ref.shape[1])
-    for out_ref, core in ((send_ref, 1 - c), (keep_ref, c)):
-        rows = [
-            branch_ref[pl.ds(pl.multiple_of((2 * x + core) * share, share), share), :]
-            for x in range(keep_ref.shape[0])
-        ]
-        out = last_dims(jnp.concatenate(rows, axis=0), weight)
-        out_ref[...] = out.astype(bf16).reshape(out_ref.shape)
-
-
-def project(place, branch, weight, share):
+    out = last_dims(
+        jnp.concatenate(rows, axis=0), weight_ref[...].reshape(-1, branch_ref.shape[1])
+    )
+    out_ref[...] = out.astype(bf16).reshape(out_ref.shape)
+
+
+def project(place, branch, pieces, share):
     width = branch.shape[1]
-    features = weight.size // width
-    half = jax.ShapeDtypeStruct((branch.shape[0] // (2 * share), share, features), bf16)
+    features = 4 * pieces[0].size // width
     return pl.pallas_call(
         project_kernel,
-        out_shape=(half, half),
-        in_specs=[SMEM, VMEM, ANY],
-        out_specs=(VMEM, VMEM),
+        out_shape=jax.ShapeDtypeStruct((branch.shape[0] // (2 * share), share, features), bf16),
+        in_specs=[SMEM, VMEM] + [ANY] * 5,
+        out_specs=VMEM,
         scratch_shapes=[
             pltpu.VMEM((2, 4, 4, features // 32, width), bf16),
-            pltpu.SemaphoreType.DMA((8,)),
+            pltpu.SemaphoreType.DMA((10,)),
         ],
         name="project",
         compiler_params=pltpu.CompilerParams(vmem_limit_bytes=16 << 20),
-    )(place, branch, weight)
+    )(place, branch, *pieces)
 
 
 def norm_rows(parts_hbm, residual_ref, gain_ref, parts_ref, sem):
@@ -218,7 +222,7 @@
         out_specs=(VMEM, VMEM, VMEM),
         scratch_shapes=[pltpu.SemaphoreType.DMA((16,))],
         name="stage",
-        compiler_params=pltpu.CompilerParams(vmem_limit_bytes=20 << 20),
+        compiler_params=pltpu.CompilerParams(vmem_limit_bytes=46 << 20),
     )(place, fed)
 
 
@@ -253,6 +257,13 @@
 
 def sideways(value, by):
     return lax.ppermute(value, "y", [(i, (i + by) % 4) for i in range(4)])
+
+
+def round_y(line):
+    after, before = sideways(line, 1), sideways(line, -1)
+    middle = line.shape[0] // 2
+    far = sideways(after[:middle], 1), sideways(before[middle:], -1)
+    return (line, after, before, *far)
 
 
 def sum_at_owner(keep, send):
@@ -280,7 +291,9 @@
     share = length // 8
     r = lax.axis_index("r")
     x, c = lax.axis_index("x"), lax.axis_index("c")
-    place = jnp.stack([c, lax.axis_index("y")]).astype(jnp.int32)
+    y = lax.axis_index("y")
+    place = jnp.stack([c, y]).astype(jnp.int32)
+    partner = jnp.stack([1 - c, y]).astype(jnp.int32)
     channels = recurrence_branch_weight.shape[1]
 
     down = feedforward_down_weight.T
@@ -292,6 +305,7 @@
         ],
         axis=0,
     )
+    fed = lax.optimization_barrier(fed)
     moved = [sideways(fed, by) for by in (1, -1, 2)]
     fed_column = jnp.stack([fed, *moved])
     fed_all = lax.all_gather(fed_column, AROUND, axis=0, tiled=False)
@@ -302,10 +316,11 @@
     )
     pair = copy_for_each(first, "zh")
     line = copy_for_each(pair, "zl")
-    branch_weight = copy_for_each(line[..., : 2 * channels], "y")
-    output_weight = copy_for_each(line[..., 2 * channels :], "y")
+    branch_weight = round_y(line[..., : 2 * channels])
+    output_weight = round_y(line[..., 2 * channels :])
 
     branch = mix(
+        place,
         tokens,
         branch_weight,
         convolution_kernel,
@@ -314,7 +329,8 @@
         channel_decay_param,
         token_decay_shift,
     )
-    mixed = sum_at_owner(*project(place, branch, output_weight, share))
+    send = project(partner, branch, output_weight, share)
+    mixed = sum_at_owner(project(place, branch, output_weight, share), send)
     own_tokens = lax.dynamic_slice_in_dim(tokens, (2 * x + c) * share, share, 0)
     normed, copies = norm(mixed, own_tokens, first_norm_gain, True)
     mine = lax.all_to_all(copies, "x", 0, 0, tiled=True)

time: 210 us -> 202 us (0.962)
  the two profiles are of different devices: /device:TPU:288 before, /device:TPU:1 now
where the time goes in v1:
time: 202 us; the launch traced here: 200 us
  blocking collectives  78.5 us (39%)
  starting transfers between devices  55.8 us (28%)
  waiting for transfers between devices  21.3 us (11%)
  Pallas kernels  20.9 us (10%)
  between operations  13.8 us (7%)
  other arithmetic  5.16 us (3%)
  local copies, waits for them, and re-layouts  4.26 us (2%)
    all_to_all x2, blocking collectives, copy_for_each(): return lax.all_to_all(copies, axis, split_axis=0, concat_axis=0, tiled=True)  45.5 us
    ppermute x11, starting transfers between devices, sideways(): return lax.ppermute(value, 'y', [(i, (i + by) % 4) for i in range(4)])  34.2 us
    ppermute x3, starting transfers between devices, to_partner(): return lax.ppermute(value, 'c', [(0, 1), (1, 0)])  17.4 us
    all_to_all x1, blocking collectives, sum_at_owner(): return lax.all_to_all(both, 'x', 0, 0, tiled=True)  17.1 us
    all_to_all x1, blocking collectives, local(): mine = lax.all_to_all(copies, 'x', 0, 0, tiled=True)  15.8 us
    all_to_all x1, waiting for transfers between devices, sum_at_owner(): return lax.all_to_all(both, 'x', 0, 0, tiled=True)  13.6 us
    ppermute x11, waiting for transfers between devices, sideways(): return lax.ppermute(value, 'y', [(i, (i + by) % 4) for i in range(4)])  7.05 us
    pallas_call x1, Pallas kernels, mix(): pl.pallas_call(mix_kernel, out_shape=jax.ShapeDtypeStruct((length, width)...  6.88 us
  transfers between devices with their start and end apart: 16, of which 5 were waited for; matrix products, arithmetic and copies ran while one was open for 2% of the time, Pallas kernels for 9%

profile of v1, /device:TPU:1, one launch (start us, length us, event | category | flops | bytes accessed | tf_op | source)
XLA Modules:
  0.0 199.8 jit_solution(3160054138621731786)
XLA Ops:
  8.3 5.6 %collective-permute-start.11 = (bf16[96,640]{1,0:T(8,128)(2,1)S(1)}, bf16[96,640]{1,0:T(8,128)(2,1)S(1)}, u32[]{:S(2)}, u32[]{:S(2)}) collective-permute-start(bf16[96,640]{1,0:T(8,128)(2,1)S(1)} %pad_maximum_fusion.1), channel_id=1, source_target_pairs={{0,16},{8,24},{16,0},{24,8},{1,17},{9,25},{17,1},{25,9},{2,18},{10... | collective-permute-start | bytes 368648 | tf_op jit(solution)/shard_map/ppermute | solution.py:259
  13.9 2.7 %collective-permute-start.10 = (bf16[96,640]{1,0:T(8,128)(2,1)S(1)}, bf16[96,640]{1,0:T(8,128)(2,1)S(1)}, u32[]{:S(2)}, u32[]{:S(2)}) collective-permute-start(bf16[96,640]{1,0:T(8,128)(2,1)S(1)} %pad_maximum_fusion.1), channel_id=1, source_target_pairs={{0,24},{8,0},{16,8},{24,16},{1,25},{9,1},{17,9},{25,17},{2,26},{10... | collective-permute-start | bytes 368648 | tf_op jit(solution)/shard_map/ppermute | solution.py:259
  16.6 2.6 %collective-permute-start.9 = (bf16[96,640]{1,0:T(8,128)(2,1)S(1)}, bf16[96,640]{1,0:T(8,128)(2,1)S(1)}, u32[]{:S(2)}, u32[]{:S(2)}) collective-permute-start(bf16[96,640]{1,0:T(8,128)(2,1)S(1)} %pad_maximum_fusion.1), channel_id=1, source_target_pairs={{0,8},{8,16},{16,24},{24,0},{1,9},{9,17},{17,25},{25,1},{2,10},{10... | collective-permute-start | bytes 368648 | tf_op jit(solution)/shard_map/ppermute | solution.py:259
  19.6 4.8 %collective-permute-done.9 = bf16[96,640]{1,0:T(8,128)(2,1)S(1)} collective-permute-done((bf16[96,640]{1,0:T(8,128)(2,1)S(1)}, bf16[96,640]{1,0:T(8,128)(2,1)S(1)}, u32[]{:S(2)}, u32[]{:S(2)}) %collective-permute-start.9) | collective-permute-done | bytes 122912 | tf_op jit(solution)/shard_map/ppermute | solution.py:259
  25.4 14.6 %all_to_all.25 = bf16[2,64,768]{2,1,0:T(8,128)(2,1)S(1)} all-to-all(bf16[2,64,768]{2,1,0:T(8,128)(2,1)S(1)} %broadcast_in_dim.6), channel_id=1, replica_groups=mesh['r'=2,'zh'=2,'zl'=4,'y'=4,'x'=4,'c'=2] {'zh'}, dimensions={0} | all-to-all | bytes 393216 | tf_op jit(solution)/shard_map/all_to_all | solution.py:21
  40.0 30.9 %all_to_all.26 = bf16[4,2,64,768]{3,2,1,0:T(8,128)(2,1)S(1)} all-to-all(bf16[4,2,64,768]{3,2,1,0:T(8,128)(2,1)S(1)} %broadcast_in_dim.7), channel_id=1, replica_groups=mesh['r'=2,'zh'=2,'zl'=4,'y'=4,'x'=4,'c'=2] {'zl'}, dimensions={0} | all-to-all | bytes 1572864 | tf_op jit(solution)/shard_map/all_to_all | solution.py:21
  71.0 1.9 collective-permute-start.1
  73.0 3.4 %collective-permute-start = (bf16[4,2,64,512]{3,2,1,0:T(8,128)(2,1)S(1)}, bf16[4,2,64,512]{3,2,1,0:T(8,128)(2,1)S(1)}, u32[]{:S(2)}, u32[]{:S(2)}) collective-permute-start(bf16[4,2,64,512]{3,2,1,0:T(8,128)(2,1)S(1)} %slice.32.refs_0_), channel_id=1, source_target_pairs={{0,8},{8,16},{16,24},{24,0},{1,9},{9,17},{17,25},{25,1},{2,10},{10... | collective-permute-start | bytes 1572872 | tf_op jit(solution)/shard_map/ppermute | solution.py:259
  76.3 3.1 %collective-permute-start.5 = (bf16[4,2,64,256]{3,2,1,0:T(8,128)(2,1)S(1)}, bf16[4,2,64,256]{3,2,1,0:T(8,128)(2,1)S(1)}, u32[]{:S(2)}, u32[]{:S(2)}) collective-permute-start(bf16[4,2,64,256]{3,2,1,0:T(8,128)(2,1)S(1)} %slice.35.refs_0_), channel_id=1, source_target_pairs={{0,24},{8,0},{16,8},{24,16},{1,25},{9,1},{17,9},{25,17},{2,26},{10... | collective-permute-start | bytes 786440 | tf_op jit(solution)/shard_map/ppermute | solution.py:259
  79.5 2.2 %collective-permute-start.4 = (bf16[4,2,64,256]{3,2,1,0:T(8,128)(2,1)S(1)}, bf16[4,2,64,256]{3,2,1,0:T(8,128)(2,1)S(1)}, u32[]{:S(2)}, u32[]{:S(2)}) collective-permute-start(bf16[4,2,64,256]{3,2,1,0:T(8,128)(2,1)S(1)} %slice.35.refs_0_), channel_id=1, source_target_pairs={{0,8},{8,16},{16,24},{24,0},{1,9},{9,17},{17,25},{25,1},{2,10},{10... | collective-permute-start | bytes 786440 | tf_op jit(solution)/shard_map/ppermute | solution.py:259
  81.7 4.3 %collective-permute-start.3 = (bf16[2,2,64,512]{3,2,1,0:T(8,128)(2,1)S(1)}, bf16[2,2,64,512]{3,2,1,0:T(8,128)(2,1)S(1)}, u32[]{:S(2)}, u32[]{:S(2)}) collective-permute-start(bf16[2,2,64,512]{3,2,1,0:T(8,128)(2,1)S(1)} %slice.34), channel_id=1, source_target_pairs={{0,24},{8,0},{16,8},{24,16},{1,25},{9,1},{17,9},{25,17},{2,26},{10... | collective-permute-start | bytes 786440 | tf_op jit(solution)/shard_map/ppermute | solution.py:259
  86.9 1.9 collective-permute-start.2
  88.8 4.6 %collective-permute-start.7 = (bf16[2,2,64,256]{3,2,1,0:T(8,128)(2,1)S(1)}, bf16[2,2,64,256]{3,2,1,0:T(8,128)(2,1)S(1)}, u32[]{:S(2)}, u32[]{:S(2)}) collective-permute-start(bf16[2,2,64,256]{3,2,1,0:T(8,128)(2,1)S(1)} %slice.37), channel_id=1, source_target_pairs={{0,24},{8,0},{16,8},{24,16},{1,25},{9,1},{17,9},{25,17},{2,26},{10... | collective-permute-start | bytes 393224 | tf_op jit(solution)/shard_map/ppermute | solution.py:259
  99.3 6.9 %mix.1.branch_ref = bf16[512,256]{1,0:T(8,128)(2,1)} custom-call(s32[2]{0:T(128)} %pad_add_fusion.place_ref, bf16[512,2048]{1,0:T(8,128)(2,1)} %tokens_hbm.1, bf16[4,2,64,512]{3,2,1,0:T(8,128)(2,1)} %copy-done.5, bf16[4,2,64,512]{3,2,1,0:T(8,128)(2,1)} %copy-done.7, bf16[4,2,64,512]{3,2,1,0:T(8,128)(2,1)} %copy-done.6, bf16[2,2,64,512]{3,2,1,0:T(8,128)(2,1)} %copy-done.9, ...), custom_call_target="tpu_custom_call" | custom-call | tf_op jit(solution)/shard_map/mix/pallas_call | solution.py:103
  108.7 10.9 %collective-permute-start.8 = (bf16[4,64,2048]{2,1,0:T(8,128)(2,1)S(1)}, bf16[4,64,2048]{2,1,0:T(8,128)(2,1)S(1)}, u32[]{:S(2)}, u32[]{:S(2)}) collective-permute-start(bf16[4,64,2048]{2,1,0:T(8,128)(2,1)S(1)} %project.3), channel_id=1, source_target_pairs={{0,1},{1,0},{2,3},{3,2},{4,5},{5,4},{6,7},{7,6},{8,9},{9,8},{10,11... | collective-permute-start | bytes 3145736 | tf_op jit(solution)/shard_map/ppermute | solution.py:255
  123.4 4.2 %all-to-all-start.2 = ((bf16[4,64,2048]{2,1,0:T(8,128)(2,1)}), bf16[4,64,2048]{2,1,0:T(8,128)(2,1)S(1)}, u32[]{:S(2)}, u32[]{:S(2)}) async-start(bf16[4,64,2048]{2,1,0:T(8,128)(2,1)} %add_convert_fusion.1), calls=%async_computation.2 | async-start | bytes 2097152 | tf_op jit(solution)/shard_map/all_to_all | solution.py:271
  128.5 13.6 %all-to-all-done.2.parts_hbm = bf16[4,64,2048]{2,1,0:T(8,128)(2,1)S(1)} async-done(((bf16[4,64,2048]{2,1,0:T(8,128)(2,1)}), bf16[4,64,2048]{2,1,0:T(8,128)(2,1)S(1)}, u32[]{:S(2)}, u32[]{:S(2)}) %all-to-all-start.2) | async-done | bytes 1048608 | tf_op jit(solution)/shard_map/all_to_all | solution.py:271
  142.6 15.8 %all_to_all.27.rows_hbm = bf16[4,64,2048]{2,1,0:T(8,128)(2,1)S(1)} all-to-all(bf16[4,64,2048]{2,1,0:T(8,128)(2,1)S(1)} %get-tuple-element.10), channel_id=1, replica_groups=mesh['r'=2,'zh'=2,'zl'=4,'y'=4,'x'=4,'c'=2] {'x'}, dimensions={0} | all-to-all | bytes 2097152 | tf_op jit(solution)/shard_map/all_to_all | solution.py:336
  158.4 4.5 %collective-permute-start.12 = (bf16[4,64,2048]{2,1,0:T(8,128)(2,1)S(1)}, bf16[4,64,2048]{2,1,0:T(8,128)(2,1)S(1)}, u32[]{:S(2)}, u32[]{:S(2)}) collective-permute-start(bf16[4,64,2048]{2,1,0:T(8,128)(2,1)S(1)} %all_to_all.27.rows_hbm), channel_id=1, source_target_pairs={{0,1},{1,0},{2,3},{3,2},{4,5},{5,4},{6,7},{7,6},{8,9},{9,8},{10,11... | collective-permute-start | bytes 3145736 | tf_op jit(solution)/shard_map/ppermute | solution.py:255
  163.0 3.9 %stage.1 = (bf16[8,4,64,640]{3,2,1,0:T(8,128)(2,1)S(1)}, bf16[8,4,64,640]{3,2,1,0:T(8,128)(2,1)S(1)}, bf16[8,4,2,32,640]{4,3,2,1,0:T(8,128)(2,1)S(1)}) custom-call(s32[2]{0:T(128)S(1)} %copy-done.4, bf16[2,8,4,96,640]{4,3,2,1,0:T(8,128)(2,1)} %bitcast.17), custom_call_target="tpu_custom_call" | custom-call | tf_op jit(solution)/shard_map/stage/pallas_call | solution.py:218
  166.9 2.7 %feed.3 = bf16[4,64,2048]{2,1,0:T(8,128)(2,1)S(1)} custom-call(bf16[4,64,2048]{2,1,0:T(8,128)(2,1)S(1)} %collective-permute-done.12.rows_hbm, bf16[8,4,64,640]{3,2,1,0:T(8,128)(2,1)S(1)} %get-tuple-element.11.gate_ref, bf16[8,4,64,640]{3,2,1,0:T(8,128)(2,1)S(1)} %get-tuple-element.12.up_ref, bf16[8,4,2,32,640]{4,3,2,1,0:T(8,128)(2,1)S(1)} %get-tuple-element.13.down_ref), custom_call_target="tpu_custom_call" | custom-call | tf_op jit(solution)/shard_map/feed/pallas_call | solution.py:243
  169.6 1.9 collective-permute-start.13
  171.5 2.7 %feed.2 = bf16[4,64,2048]{2,1,0:T(8,128)(2,1)S(1)} custom-call(bf16[4,64,2048]{2,1,0:T(8,128)(2,1)S(1)} %all_to_all.27.rows_hbm, bf16[8,4,64,640]{3,2,1,0:T(8,128)(2,1)S(1)} %get-tuple-element.11.gate_ref, bf16[8,4,64,640]{3,2,1,0:T(8,128)(2,1)S(1)} %get-tuple-element.12.up_ref, bf16[8,4,2,32,640]{4,3,2,1,0:T(8,128)(2,1)S(1)} %get-tuple-element.13.down_ref), custom_call_target="tpu_custom_call" | custom-call | tf_op jit(solution)/shard_map/feed/pallas_call | solution.py:243
  174.6 17.1 %all_to_all.28.parts_hbm = bf16[4,64,2048]{2,1,0:T(8,128)(2,1)S(1)} all-to-all(bf16[4,64,2048]{2,1,0:T(8,128)(2,1)S(1)} %add_convert_fusion), channel_id=1, replica_groups=mesh['r'=2,'zh'=2,'zl'=4,'y'=4,'x'=4,'c'=2] {'x'}, dimensions={0} | all-to-all | bytes 2097152 | tf_op jit(solution)/shard_map/all_to_all | solution.py:271
  (65 shorter events, 19.0 us)
Async XLA Ops:
  6.5 18.8 %copy-start.10 = (bf16[256,64]{0,1:T(8,128)(2,1)S(1)}, bf16[256,64]{0,1:T(8,128)(2,1)}, u32[]{:S(2)}) copy-start(bf16[256,64]{0,1:T(8,128)(2,1)} %param.22) | copy-start | bytes 98308
  6.5 18.8 %copy-start.11 = (bf16[64,256]{1,0:T(8,128)(2,1)S(1)}, bf16[64,256]{1,0:T(8,128)(2,1)}, u32[]{:S(2)}) copy-start(bf16[64,256]{1,0:T(8,128)(2,1)} %param.16) | copy-start | bytes 98308
  6.5 18.8 %copy-start.12 = (bf16[64,256]{1,0:T(8,128)(2,1)S(1)}, bf16[64,256]{1,0:T(8,128)(2,1)}, u32[]{:S(2)}) copy-start(bf16[64,256]{1,0:T(8,128)(2,1)} %param.15) | copy-start | bytes 98308
  6.5 156.4 %all-gather.3.cloned.1.call-start = ((), (), s32[]{:S(2)}) async-start(), calls=%async_computation.5 | async-start | bytes 8355840 | tf_op jit(solution)/shard_map/all_gather | solution.py:311
  8.3 10.9 %collective-permute-start.11 = (bf16[96,640]{1,0:T(8,128)(2,1)S(1)}, bf16[96,640]{1,0:T(8,128)(2,1)S(1)}, u32[]{:S(2)}, u32[]{:S(2)}) collective-permute-start(bf16[96,640]{1,0:T(8,128)(2,1)S(1)} %pad_maximum_fusion.1), channel_id=1, source_target_pairs={{0,16},{8,24},{16,0},{24,8},{1,17},{9,25},{17,1},{25,9},{2,18},{10... | collective-permute-start | bytes 368648 | tf_op jit(solution)/shard_map/ppermute | solution.py:259
  13.9 5.6 %collective-permute-start.10 = (bf16[96,640]{1,0:T(8,128)(2,1)S(1)}, bf16[96,640]{1,0:T(8,128)(2,1)S(1)}, u32[]{:S(2)}, u32[]{:S(2)}) collective-permute-start(bf16[96,640]{1,0:T(8,128)(2,1)S(1)} %pad_maximum_fusion.1), channel_id=1, source_target_pairs={{0,24},{8,0},{16,8},{24,16},{1,25},{9,1},{17,9},{25,17},{2,26},{10... | collective-permute-start | bytes 368648 | tf_op jit(solution)/shard_map/ppermute | solution.py:259
  16.6 7.8 %collective-permute-start.9 = (bf16[96,640]{1,0:T(8,128)(2,1)S(1)}, bf16[96,640]{1,0:T(8,128)(2,1)S(1)}, u32[]{:S(2)}, u32[]{:S(2)}) collective-permute-start(bf16[96,640]{1,0:T(8,128)(2,1)S(1)} %pad_maximum_fusion.1), channel_id=1, source_target_pairs={{0,8},{8,16},{16,24},{24,0},{1,9},{9,17},{17,25},{25,1},{2,10},{10... | collective-permute-start | bytes 368648 | tf_op jit(solution)/shard_map/ppermute | solution.py:259
  71.0 27.6 %copy-start.5 = (bf16[4,2,64,512]{3,2,1,0:T(8,128)(2,1)}, bf16[4,2,64,512]{3,2,1,0:T(8,128)(2,1)S(1)}, u32[]{:S(2)}) copy-start(bf16[4,2,64,512]{3,2,1,0:T(8,128)(2,1)S(1)} %slice.32.refs_0_) | copy-start | bytes 1572868
  71.0 10.6 %collective-permute-start.1 = (bf16[4,2,64,512]{3,2,1,0:T(8,128)(2,1)S(1)}, bf16[4,2,64,512]{3,2,1,0:T(8,128)(2,1)S(1)}, u32[]{:S(2)}, u32[]{:S(2)}) collective-permute-start(bf16[4,2,64,512]{3,2,1,0:T(8,128)(2,1)S(1)} %slice.32.refs_0_), channel_id=1, source_target_pairs={{0,24},{8,0},{16,8},{24,16},{1,25},{9,1},{17,9},{25,17},{2,26},{10... | collective-permute-start | bytes 1572872 | tf_op jit(solution)/shard_map/ppermute | solution.py:259
  73.0 13.1 %collective-permute-start = (bf16[4,2,64,512]{3,2,1,0:T(8,128)(2,1)S(1)}, bf16[4,2,64,512]{3,2,1,0:T(8,128)(2,1)S(1)}, u32[]{:S(2)}, u32[]{:S(2)}) collective-permute-start(bf16[4,2,64,512]{3,2,1,0:T(8,128)(2,1)S(1)} %slice.32.refs_0_), channel_id=1, source_target_pairs={{0,8},{8,16},{16,24},{24,0},{1,9},{9,17},{17,25},{25,1},{2,10},{10... | collective-permute-start | bytes 1572872 | tf_op jit(solution)/shard_map/ppermute | solution.py:259
  76.3 12.4 %collective-permute-start.5 = (bf16[4,2,64,256]{3,2,1,0:T(8,128)(2,1)S(1)}, bf16[4,2,64,256]{3,2,1,0:T(8,128)(2,1)S(1)}, u32[]{:S(2)}, u32[]{:S(2)}) collective-permute-start(bf16[4,2,64,256]{3,2,1,0:T(8,128)(2,1)S(1)} %slice.35.refs_0_), channel_id=1, source_target_pairs={{0,24},{8,0},{16,8},{24,16},{1,25},{9,1},{17,9},{25,17},{2,26},{10... | collective-permute-start | bytes 786440 | tf_op jit(solution)/shard_map/ppermute | solution.py:259
  79.5 13.9 %collective-permute-start.4 = (bf16[4,2,64,256]{3,2,1,0:T(8,128)(2,1)S(1)}, bf16[4,2,64,256]{3,2,1,0:T(8,128)(2,1)S(1)}, u32[]{:S(2)}, u32[]{:S(2)}) collective-permute-start(bf16[4,2,64,256]{3,2,1,0:T(8,128)(2,1)S(1)} %slice.35.refs_0_), channel_id=1, source_target_pairs={{0,8},{8,16},{16,24},{24,0},{1,9},{9,17},{17,25},{25,1},{2,10},{10... | collective-permute-start | bytes 786440 | tf_op jit(solution)/shard_map/ppermute | solution.py:259
  81.7 16.9 %copy-start.6 = (bf16[4,2,64,512]{3,2,1,0:T(8,128)(2,1)}, bf16[4,2,64,512]{3,2,1,0:T(8,128)(2,1)S(1)}, u32[]{:S(2)}) copy-start(bf16[4,2,64,512]{3,2,1,0:T(8,128)(2,1)S(1)} %collective-permute-done.1.refs_2_) | copy-start | bytes 1572868
  81.7 15.0 %collective-permute-start.3 = (bf16[2,2,64,512]{3,2,1,0:T(8,128)(2,1)S(1)}, bf16[2,2,64,512]{3,2,1,0:T(8,128)(2,1)S(1)}, u32[]{:S(2)}, u32[]{:S(2)}) collective-permute-start(bf16[2,2,64,512]{3,2,1,0:T(8,128)(2,1)S(1)} %slice.34), channel_id=1, source_target_pairs={{0,24},{8,0},{16,8},{24,16},{1,25},{9,1},{17,9},{25,17},{2,26},{10... | collective-permute-start | bytes 786440 | tf_op jit(solution)/shard_map/ppermute | solution.py:259
  86.9 11.7 %collective-permute-start.2 = (bf16[2,2,64,512]{3,2,1,0:T(8,128)(2,1)}, bf16[2,2,64,512]{3,2,1,0:T(8,128)(2,1)S(1)}, u32[]{:S(2)}, u32[]{:S(2)}) collective-permute-start(bf16[2,2,64,512]{3,2,1,0:T(8,128)(2,1)} %slice.33), channel_id=1, source_target_pairs={{0,8},{8,16},{16,24},{24,0},{1,9},{9,17},{17,25},{25,1},{2,10},{10... | collective-permute-start | bytes 786440 | tf_op jit(solution)/shard_map/ppermute | solution.py:259
  88.8 17.4 %collective-permute-start.7 = (bf16[2,2,64,256]{3,2,1,0:T(8,128)(2,1)S(1)}, bf16[2,2,64,256]{3,2,1,0:T(8,128)(2,1)S(1)}, u32[]{:S(2)}, u32[]{:S(2)}) collective-permute-start(bf16[2,2,64,256]{3,2,1,0:T(8,128)(2,1)S(1)} %slice.37), channel_id=1, source_target_pairs={{0,24},{8,0},{16,8},{24,16},{1,25},{9,1},{17,9},{25,17},{2,26},{10... | collective-permute-start | bytes 393224 | tf_op jit(solution)/shard_map/ppermute | solution.py:259
  94.1 12.1 %collective-permute-start.6 = (bf16[2,2,64,256]{3,2,1,0:T(8,128)(2,1)}, bf16[2,2,64,256]{3,2,1,0:T(8,128)(2,1)S(1)}, u32[]{:S(2)}, u32[]{:S(2)}) collective-permute-start(bf16[2,2,64,256]{3,2,1,0:T(8,128)(2,1)} %slice.36), channel_id=1, source_target_pairs={{0,8},{8,16},{16,24},{24,0},{1,9},{9,17},{17,25},{25,1},{2,10},{10... | collective-permute-start | bytes 393224 | tf_op jit(solution)/shard_map/ppermute | solution.py:259
  99.3 20.4 %copy-start.4 = (s32[2]{0:T(128)S(1)}, s32[2]{0:T(128)}, u32[]{:S(2)}) copy-start(s32[2]{0:T(128)} %pad_add_fusion.place_ref) | copy-start | bytes 28
  108.7 13.2 %collective-permute-start.8 = (bf16[4,64,2048]{2,1,0:T(8,128)(2,1)S(1)}, bf16[4,64,2048]{2,1,0:T(8,128)(2,1)S(1)}, u32[]{:S(2)}, u32[]{:S(2)}) collective-permute-start(bf16[4,64,2048]{2,1,0:T(8,128)(2,1)S(1)} %project.3), channel_id=1, source_target_pairs={{0,1},{1,0},{2,3},{3,2},{4,5},{5,4},{6,7},{7,6},{8,9},{9,8},{10,11... | collective-permute-start | bytes 3145736 | tf_op jit(solution)/shard_map/ppermute | solution.py:255
  123.4 18.7 %copy-start.2 = (f32[2048]{0:T(1024)S(1)}, f32[2048]{0:T(1024)}, u32[]{:S(2)}) copy-start(f32[2048]{0:T(1024)} %param.23) | copy-start | bytes 24580
  123.4 18.7 %all-to-all-start.2 = ((bf16[4,64,2048]{2,1,0:T(8,128)(2,1)}), bf16[4,64,2048]{2,1,0:T(8,128)(2,1)S(1)}, u32[]{:S(2)}, u32[]{:S(2)}) async-start(bf16[4,64,2048]{2,1,0:T(8,128)(2,1)} %add_convert_fusion.1), calls=%async_computation.2 | async-start | bytes 2097152 | tf_op jit(solution)/shard_map/all_to_all | solution.py:271
  158.4 8.5 %collective-permute-start.12 = (bf16[4,64,2048]{2,1,0:T(8,128)(2,1)S(1)}, bf16[4,64,2048]{2,1,0:T(8,128)(2,1)S(1)}, u32[]{:S(2)}, u32[]{:S(2)}) collective-permute-start(bf16[4,64,2048]{2,1,0:T(8,128)(2,1)S(1)} %all_to_all.27.rows_hbm), channel_id=1, source_target_pairs={{0,1},{1,0},{2,3},{3,2},{4,5},{5,4},{6,7},{7,6},{8,9},{9,8},{10,11... | collective-permute-start | bytes 3145736 | tf_op jit(solution)/shard_map/ppermute | solution.py:255
  169.6 4.6 %collective-permute-start.13 = (bf16[4,64,2048]{2,1,0:T(8,128)(2,1)S(1)}, bf16[4,64,2048]{2,1,0:T(8,128)(2,1)S(1)}, u32[]{:S(2)}, u32[]{:S(2)}) collective-permute-start(bf16[4,64,2048]{2,1,0:T(8,128)(2,1)S(1)} %feed.3), channel_id=1, source_target_pairs={{0,1},{1,0},{2,3},{3,2},{4,5},{5,4},{6,7},{7,6},{8,9},{9,8},{10,11... | collective-permute-start | bytes 3145736 | tf_op jit(solution)/shard_map/ppermute | solution.py:255
  174.2 17.5 %copy-start.3 = (f32[2048]{0:T(1024)S(1)}, f32[2048]{0:T(1024)}, u32[]{:S(2)}) copy-start(f32[2048]{0:T(1024)} %param.27) | copy-start | bytes 24580
  (5 other events, 28.6 us)
Sparse Core Ops, SparseCore 0:
  25.4 116.7 all-gather.2

commit v2 on v1

--- a/solution.py
+++ b/solution.py
@@ -114,7 +114,7 @@
             pltpu.SemaphoreType.DMA((12,)),
         ],
         name="mix",
-        compiler_params=pltpu.CompilerParams(vmem_limit_bytes=60 << 20),
+        compiler_params=pltpu.CompilerParams(vmem_limit_bytes=16 << 20),
     )(place, tokens, *pieces, taps, rec, inp, decay.reshape(1, width), shift)
 
 
@@ -122,12 +122,15 @@
     return lax.dot_general(left, right, (((1,), (1,)), ((), ())), preferred_element_type=f32)
 
 
-def project_kernel(place_ref, branch_ref, *refs):
-    pieces, (out_ref, weight_ref, sems) = refs[:5], refs[5:]
+def project_kernel(place_ref, branch_hbm, *refs):
+    pieces, (out_ref, branch_ref, weight_ref, sems) = refs[:5], refs[5:]
     core = place_ref[0]
     copies = loads(pieces, weight_ref, place_ref[1], sems)
+    whole = pltpu.make_async_copy(branch_hbm, branch_ref, sems.at[len(copies)])
+    whole.start()
     start_all(copies)
     share = out_ref.shape[1]
+    whole.wait()
     rows = [
         branch_ref[pl.ds(pl.multiple_of((2 * x + core) * share, share), share), :]
         for x in range(out_ref.shape[0])
@@ -145,11 +148,12 @@
     return pl.pallas_call(
         project_kernel,
         out_shape=jax.ShapeDtypeStruct((branch.shape[0] // (2 * share), share, features), bf16),
-        in_specs=[SMEM, VMEM] + [ANY] * 5,
+        in_specs=[SMEM, ANY] + [ANY] * 5,
         out_specs=VMEM,
         scratch_shapes=[
+            pltpu.VMEM(branch.shape, bf16),
             pltpu.VMEM((2, 4, 4, features // 32, width), bf16),
-            pltpu.SemaphoreType.DMA((10,)),
+            pltpu.SemaphoreType.DMA((11,)),
         ],
         name="project",
         compiler_params=pltpu.CompilerParams(vmem_limit_bytes=16 << 20),
@@ -296,6 +300,8 @@
     partner = jnp.stack([1 - c, y]).astype(jnp.int32)
     channels = recurrence_branch_weight.shape[1]
 
+    own_tokens = lax.dynamic_slice_in_dim(tokens, (2 * x + c) * share, share, 0)
+
     down = feedforward_down_weight.T
     height = down.shape[0]
     fed = jnp.concatenate(
@@ -331,7 +337,6 @@
     )
     send = project(partner, branch, output_weight, share)
     mixed = sum_at_owner(project(place, branch, output_weight, share), send)
-    own_tokens = lax.dynamic_slice_in_dim(tokens, (2 * x + c) * share, share, 0)
     normed, copies = norm(mixed, own_tokens, first_norm_gain, True)
     mine = lax.all_to_all(copies, "x", 0, 0, tiled=True)
     other = to_partner(mine)

time: 202 us -> 204 us (level)
  local copies, waits for them, and re-layouts: 4.26 us -> 8.26 us
    unnamed x26 -> x30, local copies, waits for them, and re-layouts: 1.67 us -> 5.16 us
    pallas_call x1, Pallas kernels: 6.88 us -> 4.64 us  [mix(): pl.pallas_call(mix_kernel, out_shape=jax.ShapeDtypeStruct((length, width)...]
  transfers between devices with their start and end apart: 16 -> 16, of which waited for: 5 -> 4; matrix products, arithmetic and copies ran while one was open for 2% -> 2% of each run, Pallas kernels for 9% -> 8%
where the time goes in v2:
time: 204 us; the launch traced here: 202 us
  blocking collectives  78.7 us (39%)
  starting transfers between devices  54.8 us (27%)
  waiting for transfers between devices  21.5 us (11%)
  Pallas kernels  20.1 us (10%)
  between operations  13.8 us (7%)
  local copies, waits for them, and re-layouts  8.26 us (4%)
  other arithmetic  4.59 us (2%)
    all_to_all x2, blocking collectives, copy_for_each(): return lax.all_to_all(copies, axis, split_axis=0, concat_axis=0, tiled=True)  45.7 us
    ppermute x11, starting transfers between devices, sideways(): return lax.ppermute(value, 'y', [(i, (i + by) % 4) for i in range(4)])  34.2 us
    all_to_all x1, blocking collectives, sum_at_owner(): return lax.all_to_all(both, 'x', 0, 0, tiled=True)  17.1 us
    ppermute x3, starting transfers between devices, to_partner(): return lax.ppermute(value, 'c', [(0, 1), (1, 0)])  16.5 us
    all_to_all x1, blocking collectives, local(): mine = lax.all_to_all(copies, 'x', 0, 0, tiled=True)  15.8 us
    all_to_all x1, waiting for transfers between devices, sum_at_owner(): return lax.all_to_all(both, 'x', 0, 0, tiled=True)  14.5 us
    ppermute x11, waiting for transfers between devices, sideways(): return lax.ppermute(value, 'y', [(i, (i + by) % 4) for i in range(4)])  6.87 us
    pallas_call x2, Pallas kernels, feed(): pl.pallas_call(feed_kernel, out_shape=jax.ShapeDtypeStruct(rows.shape, bf...  5.4 us
  transfers between devices with their start and end apart: 16, of which 4 were waited for; matrix products, arithmetic and copies ran while one was open for 2% of the time, Pallas kernels for 8%

profile of v2, /device:TPU:1, one launch (start us, length us, event | category | flops | bytes accessed | tf_op | source)
XLA Modules:
  0.0 201.7 jit_solution(5892515753184110686)
XLA Ops:
  8.3 5.6 %collective-permute-start.11 = (bf16[96,640]{1,0:T(8,128)(2,1)S(1)}, bf16[96,640]{1,0:T(8,128)(2,1)S(1)}, u32[]{:S(2)}, u32[]{:S(2)}) collective-permute-start(bf16[96,640]{1,0:T(8,128)(2,1)S(1)} %pad_maximum_fusion.1), channel_id=1, source_target_pairs={{0,16},{8,24},{16,0},{24,8},{1,17},{9,25},{17,1},{25,9},{2,18},{10... | collective-permute-start | bytes 368648 | tf_op jit(solution)/shard_map/ppermute | solution.py:263
  13.9 2.7 %collective-permute-start.10 = (bf16[96,640]{1,0:T(8,128)(2,1)S(1)}, bf16[96,640]{1,0:T(8,128)(2,1)S(1)}, u32[]{:S(2)}, u32[]{:S(2)}) collective-permute-start(bf16[96,640]{1,0:T(8,128)(2,1)S(1)} %pad_maximum_fusion.1), channel_id=1, source_target_pairs={{0,24},{8,0},{16,8},{24,16},{1,25},{9,1},{17,9},{25,17},{2,26},{10... | collective-permute-start | bytes 368648 | tf_op jit(solution)/shard_map/ppermute | solution.py:263
  16.6 2.6 %collective-permute-start.9 = (bf16[96,640]{1,0:T(8,128)(2,1)S(1)}, bf16[96,640]{1,0:T(8,128)(2,1)S(1)}, u32[]{:S(2)}, u32[]{:S(2)}) collective-permute-start(bf16[96,640]{1,0:T(8,128)(2,1)S(1)} %pad_maximum_fusion.1), channel_id=1, source_target_pairs={{0,8},{8,16},{16,24},{24,0},{1,9},{9,17},{17,25},{25,1},{2,10},{10... | collective-permute-start | bytes 368648 | tf_op jit(solution)/shard_map/ppermute | solution.py:263
  19.6 4.8 %collective-permute-done.9 = bf16[96,640]{1,0:T(8,128)(2,1)S(1)} collective-permute-done((bf16[96,640]{1,0:T(8,128)(2,1)S(1)}, bf16[96,640]{1,0:T(8,128)(2,1)S(1)}, u32[]{:S(2)}, u32[]{:S(2)}) %collective-permute-start.9) | collective-permute-done | bytes 122912 | tf_op jit(solution)/shard_map/ppermute | solution.py:263
  25.4 14.6 %all_to_all.25 = bf16[2,64,768]{2,1,0:T(8,128)(2,1)S(1)} all-to-all(bf16[2,64,768]{2,1,0:T(8,128)(2,1)S(1)} %broadcast_in_dim.6), channel_id=1, replica_groups=mesh['r'=2,'zh'=2,'zl'=4,'y'=4,'x'=4,'c'=2] {'zh'}, dimensions={0} | all-to-all | bytes 393216 | tf_op jit(solution)/shard_map/all_to_all | solution.py:21
  40.1 31.1 %all_to_all.26 = bf16[4,2,64,768]{3,2,1,0:T(8,128)(2,1)S(1)} all-to-all(bf16[4,2,64,768]{3,2,1,0:T(8,128)(2,1)S(1)} %broadcast_in_dim.7), channel_id=1, replica_groups=mesh['r'=2,'zh'=2,'zl'=4,'y'=4,'x'=4,'c'=2] {'zl'}, dimensions={0} | all-to-all | bytes 1572864 | tf_op jit(solution)/shard_map/all_to_all | solution.py:21
  71.2 1.9 collective-permute-start.1
  73.1 3.4 %collective-permute-start = (bf16[4,2,64,512]{3,2,1,0:T(8,128)(2,1)S(1)}, bf16[4,2,64,512]{3,2,1,0:T(8,128)(2,1)S(1)}, u32[]{:S(2)}, u32[]{:S(2)}) collective-permute-start(bf16[4,2,64,512]{3,2,1,0:T(8,128)(2,1)S(1)} %slice.32.refs_0_), channel_id=1, source_target_pairs={{0,8},{8,16},{16,24},{24,0},{1,9},{9,17},{17,25},{25,1},{2,10},{10... | collective-permute-start | bytes 1572872 | tf_op jit(solution)/shard_map/ppermute | solution.py:263
  76.5 3.1 %collective-permute-start.5 = (bf16[4,2,64,256]{3,2,1,0:T(8,128)(2,1)S(1)}, bf16[4,2,64,256]{3,2,1,0:T(8,128)(2,1)S(1)}, u32[]{:S(2)}, u32[]{:S(2)}) collective-permute-start(bf16[4,2,64,256]{3,2,1,0:T(8,128)(2,1)S(1)} %slice.35.refs_0_), channel_id=1, source_target_pairs={{0,24},{8,0},{16,8},{24,16},{1,25},{9,1},{17,9},{25,17},{2,26},{10... | collective-permute-start | bytes 786440 | tf_op jit(solution)/shard_map/ppermute | solution.py:263
  79.7 2.2 %collective-permute-start.4 = (bf16[4,2,64,256]{3,2,1,0:T(8,128)(2,1)S(1)}, bf16[4,2,64,256]{3,2,1,0:T(8,128)(2,1)S(1)}, u32[]{:S(2)}, u32[]{:S(2)}) collective-permute-start(bf16[4,2,64,256]{3,2,1,0:T(8,128)(2,1)S(1)} %slice.35.refs_0_), channel_id=1, source_target_pairs={{0,8},{8,16},{16,24},{24,0},{1,9},{9,17},{17,25},{25,1},{2,10},{10... | collective-permute-start | bytes 786440 | tf_op jit(solution)/shard_map/ppermute | solution.py:263
  82.7 4.3 %collective-permute-start.3 = (bf16[2,2,64,512]{3,2,1,0:T(8,128)(2,1)}, bf16[2,2,64,512]{3,2,1,0:T(8,128)(2,1)}, u32[]{:S(2)}, u32[]{:S(2)}) collective-permute-start(bf16[2,2,64,512]{3,2,1,0:T(8,128)(2,1)} %slice.34), channel_id=1, source_target_pairs={{0,24},{8,0},{16,8},{24,16},{1,25},{9,1},{17,9},{25,17},{2,26},{10... | collective-permute-start | bytes 786440 | tf_op jit(solution)/shard_map/ppermute | solution.py:263
  90.6 4.6 %collective-permute-start.7 = (bf16[2,2,64,256]{3,2,1,0:T(8,128)(2,1)}, bf16[2,2,64,256]{3,2,1,0:T(8,128)(2,1)S(1)}, u32[]{:S(2)}, u32[]{:S(2)}) collective-permute-start(bf16[2,2,64,256]{3,2,1,0:T(8,128)(2,1)} %slice.37), channel_id=1, source_target_pairs={{0,24},{8,0},{16,8},{24,16},{1,25},{9,1},{17,9},{25,17},{2,26},{10... | collective-permute-start | bytes 393224 | tf_op jit(solution)/shard_map/ppermute | solution.py:263
  104.6 4.6 %mix.1.branch_hbm = bf16[512,256]{1,0:T(8,128)(2,1)S(1)} custom-call(s32[2]{0:T(128)S(1)} %pad_add_fusion.place_ref, bf16[512,2048]{1,0:T(8,128)(2,1)S(1)} %copy-done, bf16[4,2,64,512]{3,2,1,0:T(8,128)(2,1)S(1)} %slice.32.refs_0_, bf16[4,2,64,512]{3,2,1,0:T(8,128)(2,1)S(1)} %copy-done.4, bf16[4,2,64,512]{3,2,1,0:T(8,128)(2,1)S(1)} %copy-done.2, ...), custom_call_target="tpu_custom_call" | custom-call | tf_op jit(solution)/shard_map/mix/pallas_call | solution.py:103
  109.3 2.3 %project.3 = bf16[4,64,2048]{2,1,0:T(8,128)(2,1)S(1)} custom-call(s32[2]{0:T(128)S(1)} %pad_add_fusion.1.place_ref, bf16[512,256]{1,0:T(8,128)(2,1)S(1)} %mix.1.branch_hbm, bf16[4,2,64,256]{3,2,1,0:T(8,128)(2,1)S(1)} %slice.35.refs_0_, bf16[4,2,64,256]{3,2,1,0:T(8,128)(2,1)S(1)} %collective-permute-done.4.refs_1_, ...), custom_call_target="tpu_custom_call" | custom-call | tf_op jit(solution)/shard_map/project/pallas_call | solution.py:148
  111.6 10.0 %collective-permute-start.8 = (bf16[4,64,2048]{2,1,0:T(8,128)(2,1)S(1)}, bf16[4,64,2048]{2,1,0:T(8,128)(2,1)S(1)}, u32[]{:S(2)}, u32[]{:S(2)}) collective-permute-start(bf16[4,64,2048]{2,1,0:T(8,128)(2,1)S(1)} %project.3), channel_id=1, source_target_pairs={{0,1},{1,0},{2,3},{3,2},{4,5},{5,4},{6,7},{7,6},{8,9},{9,8},{10,11... | collective-permute-start | bytes 3145736 | tf_op jit(solution)/shard_map/ppermute | solution.py:259
  121.6 2.3 %project.2 = bf16[4,64,2048]{2,1,0:T(8,128)(2,1)S(1)} custom-call(s32[2]{0:T(128)S(1)} %pad_add_fusion.place_ref, bf16[512,256]{1,0:T(8,128)(2,1)S(1)} %mix.1.branch_hbm, bf16[4,2,64,256]{3,2,1,0:T(8,128)(2,1)S(1)} %slice.35.refs_0_, bf16[4,2,64,256]{3,2,1,0:T(8,128)(2,1)S(1)} %collective-permute-done.4.refs_1_, ...), custom_call_target="tpu_custom_call" | custom-call | tf_op jit(solution)/shard_map/project/pallas_call | solution.py:148
  125.3 4.1 %all-to-all-start.2 = ((bf16[4,64,2048]{2,1,0:T(8,128)(2,1)}), bf16[4,64,2048]{2,1,0:T(8,128)(2,1)S(1)}, u32[]{:S(2)}, u32[]{:S(2)}) async-start(bf16[4,64,2048]{2,1,0:T(8,128)(2,1)} %add_convert_fusion.1), calls=%async_computation.2 | async-start | bytes 2097152 | tf_op jit(solution)/shard_map/all_to_all | solution.py:275
  129.5 14.5 %all-to-all-done.2.parts_hbm = bf16[4,64,2048]{2,1,0:T(8,128)(2,1)S(1)} async-done(((bf16[4,64,2048]{2,1,0:T(8,128)(2,1)}), bf16[4,64,2048]{2,1,0:T(8,128)(2,1)S(1)}, u32[]{:S(2)}, u32[]{:S(2)}) %all-to-all-start.2) | async-done | bytes 1048608 | tf_op jit(solution)/shard_map/all_to_all | solution.py:275
  144.5 15.8 %all_to_all.27.rows_hbm = bf16[4,64,2048]{2,1,0:T(8,128)(2,1)S(1)} all-to-all(bf16[4,64,2048]{2,1,0:T(8,128)(2,1)S(1)} %get-tuple-element.10), channel_id=1, replica_groups=mesh['r'=2,'zh'=2,'zl'=4,'y'=4,'x'=4,'c'=2] {'x'}, dimensions={0} | all-to-all | bytes 2097152 | tf_op jit(solution)/shard_map/all_to_all | solution.py:341
  160.4 4.5 %collective-permute-start.12 = (bf16[4,64,2048]{2,1,0:T(8,128)(2,1)S(1)}, bf16[4,64,2048]{2,1,0:T(8,128)(2,1)S(1)}, u32[]{:S(2)}, u32[]{:S(2)}) collective-permute-start(bf16[4,64,2048]{2,1,0:T(8,128)(2,1)S(1)} %all_to_all.27.rows_hbm), channel_id=1, source_target_pairs={{0,1},{1,0},{2,3},{3,2},{4,5},{5,4},{6,7},{7,6},{8,9},{9,8},{10,11... | collective-permute-start | bytes 3145736 | tf_op jit(solution)/shard_map/ppermute | solution.py:259
  164.9 3.9 %stage.1 = (bf16[8,4,64,640]{3,2,1,0:T(8,128)(2,1)S(1)}, bf16[8,4,64,640]{3,2,1,0:T(8,128)(2,1)S(1)}, bf16[8,4,2,32,640]{4,3,2,1,0:T(8,128)(2,1)S(1)}) custom-call(s32[2]{0:T(128)S(1)} %pad_add_fusion.place_ref, bf16[2,8,4,96,640]{4,3,2,1,0:T(8,128)(2,1)} %bitcast.20), custom_call_target="tpu_custom_call" | custom-call | tf_op jit(solution)/shard_map/stage/pallas_call | solution.py:222
  168.8 2.7 %feed.3 = bf16[4,64,2048]{2,1,0:T(8,128)(2,1)S(1)} custom-call(bf16[4,64,2048]{2,1,0:T(8,128)(2,1)S(1)} %collective-permute-done.12.rows_hbm, bf16[8,4,64,640]{3,2,1,0:T(8,128)(2,1)S(1)} %get-tuple-element.11.gate_ref, bf16[8,4,64,640]{3,2,1,0:T(8,128)(2,1)S(1)} %get-tuple-element.12.up_ref, bf16[8,4,2,32,640]{4,3,2,1,0:T(8,128)(2,1)S(1)} %get-tuple-element.13.down_ref), custom_call_target="tpu_custom_call" | custom-call | tf_op jit(solution)/shard_map/feed/pallas_call | solution.py:247
  173.5 2.7 %feed.2 = bf16[4,64,2048]{2,1,0:T(8,128)(2,1)S(1)} custom-call(bf16[4,64,2048]{2,1,0:T(8,128)(2,1)S(1)} %all_to_all.27.rows_hbm, bf16[8,4,64,640]{3,2,1,0:T(8,128)(2,1)S(1)} %get-tuple-element.11.gate_ref, bf16[8,4,64,640]{3,2,1,0:T(8,128)(2,1)S(1)} %get-tuple-element.12.up_ref, bf16[8,4,2,32,640]{4,3,2,1,0:T(8,128)(2,1)S(1)} %get-tuple-element.13.down_ref), custom_call_target="tpu_custom_call" | custom-call | tf_op jit(solution)/shard_map/feed/pallas_call | solution.py:247
  176.6 17.1 %all_to_all.28.parts_hbm = bf16[4,64,2048]{2,1,0:T(8,128)(2,1)S(1)} all-to-all(bf16[4,64,2048]{2,1,0:T(8,128)(2,1)S(1)} %add_convert_fusion), channel_id=1, replica_groups=mesh['r'=2,'zh'=2,'zl'=4,'y'=4,'x'=4,'c'=2] {'x'}, dimensions={0} | all-to-all | bytes 2097152 | tf_op jit(solution)/shard_map/all_to_all | solution.py:275
  (69 shorter events, 22.3 us)
Async XLA Ops:
  6.5 18.8 %copy-start.12 = (bf16[256,64]{0,1:T(8,128)(2,1)S(1)}, bf16[256,64]{0,1:T(8,128)(2,1)}, u32[]{:S(2)}) copy-start(bf16[256,64]{0,1:T(8,128)(2,1)} %param.22) | copy-start | bytes 98308
  6.5 18.8 %copy-start.13 = (bf16[64,256]{1,0:T(8,128)(2,1)S(1)}, bf16[64,256]{1,0:T(8,128)(2,1)}, u32[]{:S(2)}) copy-start(bf16[64,256]{1,0:T(8,128)(2,1)} %param.16) | copy-start | bytes 98308
  6.5 18.8 %copy-start.14 = (bf16[64,256]{1,0:T(8,128)(2,1)S(1)}, bf16[64,256]{1,0:T(8,128)(2,1)}, u32[]{:S(2)}) copy-start(bf16[64,256]{1,0:T(8,128)(2,1)} %param.15) | copy-start | bytes 98308
  6.5 158.4 %all-gather.3.cloned.1.call-start = ((), (), s32[]{:S(2)}) async-start(), calls=%async_computation.5 | async-start | bytes 8355840 | tf_op jit(solution)/shard_map/all_gather | solution.py:317
  8.3 10.9 %collective-permute-start.11 = (bf16[96,640]{1,0:T(8,128)(2,1)S(1)}, bf16[96,640]{1,0:T(8,128)(2,1)S(1)}, u32[]{:S(2)}, u32[]{:S(2)}) collective-permute-start(bf16[96,640]{1,0:T(8,128)(2,1)S(1)} %pad_maximum_fusion.1), channel_id=1, source_target_pairs={{0,16},{8,24},{16,0},{24,8},{1,17},{9,25},{17,1},{25,9},{2,18},{10... | collective-permute-start | bytes 368648 | tf_op jit(solution)/shard_map/ppermute | solution.py:263
  13.9 5.6 %collective-permute-start.10 = (bf16[96,640]{1,0:T(8,128)(2,1)S(1)}, bf16[96,640]{1,0:T(8,128)(2,1)S(1)}, u32[]{:S(2)}, u32[]{:S(2)}) collective-permute-start(bf16[96,640]{1,0:T(8,128)(2,1)S(1)} %pad_maximum_fusion.1), channel_id=1, source_target_pairs={{0,24},{8,0},{16,8},{24,16},{1,25},{9,1},{17,9},{25,17},{2,26},{10... | collective-permute-start | bytes 368648 | tf_op jit(solution)/shard_map/ppermute | solution.py:263
  16.6 7.8 %collective-permute-start.9 = (bf16[96,640]{1,0:T(8,128)(2,1)S(1)}, bf16[96,640]{1,0:T(8,128)(2,1)S(1)}, u32[]{:S(2)}, u32[]{:S(2)}) collective-permute-start(bf16[96,640]{1,0:T(8,128)(2,1)S(1)} %pad_maximum_fusion.1), channel_id=1, source_target_pairs={{0,8},{8,16},{16,24},{24,0},{1,9},{9,17},{17,25},{25,1},{2,10},{10... | collective-permute-start | bytes 368648 | tf_op jit(solution)/shard_map/ppermute | solution.py:263
  40.0 59.6 %copy-start = (bf16[512,2048]{1,0:T(8,128)(2,1)S(1)}, bf16[512,2048]{1,0:T(8,128)(2,1)}, u32[]{:S(2)}) copy-start(bf16[512,2048]{1,0:T(8,128)(2,1)} %tokens_hbm.1) | copy-start | bytes 6291460
  40.0 59.6 %copy-start.10 = (bf16[4,256]{1,0:T(4,128)(2,1)S(1)}, bf16[4,256]{1,0:T(4,128)(2,1)}, u32[]{:S(2)}) copy-start(bf16[4,256]{1,0:T(4,128)(2,1)} %refs_5_.1) | copy-start | bytes 6148
  40.1 59.6 %copy-start.11 = (f32[256]{0:T(256)S(1)}, f32[256]{0:T(256)}, u32[]{:S(2)}) copy-start(f32[256]{0:T(256)} %param.20) | copy-start | bytes 3076
  71.2 10.6 %collective-permute-start.1 = (bf16[4,2,64,512]{3,2,1,0:T(8,128)(2,1)S(1)}, bf16[4,2,64,512]{3,2,1,0:T(8,128)(2,1)S(1)}, u32[]{:S(2)}, u32[]{:S(2)}) collective-permute-start(bf16[4,2,64,512]{3,2,1,0:T(8,128)(2,1)S(1)} %slice.32.refs_0_), channel_id=1, source_target_pairs={{0,24},{8,0},{16,8},{24,16},{1,25},{9,1},{17,9},{25,17},{2,26},{10... | collective-permute-start | bytes 1572872 | tf_op jit(solution)/shard_map/ppermute | solution.py:263
  73.1 13.9 %collective-permute-start = (bf16[4,2,64,512]{3,2,1,0:T(8,128)(2,1)S(1)}, bf16[4,2,64,512]{3,2,1,0:T(8,128)(2,1)S(1)}, u32[]{:S(2)}, u32[]{:S(2)}) collective-permute-start(bf16[4,2,64,512]{3,2,1,0:T(8,128)(2,1)S(1)} %slice.32.refs_0_), channel_id=1, source_target_pairs={{0,8},{8,16},{16,24},{24,0},{1,9},{9,17},{17,25},{25,1},{2,10},{10... | collective-permute-start | bytes 1572872 | tf_op jit(solution)/shard_map/ppermute | solution.py:263
  76.5 13.4 %collective-permute-start.5 = (bf16[4,2,64,256]{3,2,1,0:T(8,128)(2,1)S(1)}, bf16[4,2,64,256]{3,2,1,0:T(8,128)(2,1)S(1)}, u32[]{:S(2)}, u32[]{:S(2)}) collective-permute-start(bf16[4,2,64,256]{3,2,1,0:T(8,128)(2,1)S(1)} %slice.35.refs_0_), channel_id=1, source_target_pairs={{0,24},{8,0},{16,8},{24,16},{1,25},{9,1},{17,9},{25,17},{2,26},{10... | collective-permute-start | bytes 786440 | tf_op jit(solution)/shard_map/ppermute | solution.py:263
  79.7 15.5 %collective-permute-start.4 = (bf16[4,2,64,256]{3,2,1,0:T(8,128)(2,1)S(1)}, bf16[4,2,64,256]{3,2,1,0:T(8,128)(2,1)S(1)}, u32[]{:S(2)}, u32[]{:S(2)}) collective-permute-start(bf16[4,2,64,256]{3,2,1,0:T(8,128)(2,1)S(1)} %slice.35.refs_0_), channel_id=1, source_target_pairs={{0,8},{8,16},{16,24},{24,0},{1,9},{9,17},{17,25},{25,1},{2,10},{10... | collective-permute-start | bytes 786440 | tf_op jit(solution)/shard_map/ppermute | solution.py:263
  82.7 15.3 %collective-permute-start.3 = (bf16[2,2,64,512]{3,2,1,0:T(8,128)(2,1)}, bf16[2,2,64,512]{3,2,1,0:T(8,128)(2,1)}, u32[]{:S(2)}, u32[]{:S(2)}) collective-permute-start(bf16[2,2,64,512]{3,2,1,0:T(8,128)(2,1)} %slice.34), channel_id=1, source_target_pairs={{0,24},{8,0},{16,8},{24,16},{1,25},{9,1},{17,9},{25,17},{2,26},{10... | collective-permute-start | bytes 786440 | tf_op jit(solution)/shard_map/ppermute | solution.py:263
  88.0 11.6 %collective-permute-start.2 = (bf16[2,2,64,512]{3,2,1,0:T(8,128)(2,1)}, bf16[2,2,64,512]{3,2,1,0:T(8,128)(2,1)}, u32[]{:S(2)}, u32[]{:S(2)}) collective-permute-start(bf16[2,2,64,512]{3,2,1,0:T(8,128)(2,1)} %slice.33), channel_id=1, source_target_pairs={{0,8},{8,16},{16,24},{24,0},{1,9},{9,17},{17,25},{25,1},{2,10},{10... | collective-permute-start | bytes 786440 | tf_op jit(solution)/shard_map/ppermute | solution.py:263
  90.6 18.6 %collective-permute-start.7 = (bf16[2,2,64,256]{3,2,1,0:T(8,128)(2,1)}, bf16[2,2,64,256]{3,2,1,0:T(8,128)(2,1)S(1)}, u32[]{:S(2)}, u32[]{:S(2)}) collective-permute-start(bf16[2,2,64,256]{3,2,1,0:T(8,128)(2,1)} %slice.37), channel_id=1, source_target_pairs={{0,24},{8,0},{16,8},{24,16},{1,25},{9,1},{17,9},{25,17},{2,26},{10... | collective-permute-start | bytes 393224 | tf_op jit(solution)/shard_map/ppermute | solution.py:263
  95.9 13.4 %collective-permute-start.6 = (bf16[2,2,64,256]{3,2,1,0:T(8,128)(2,1)}, bf16[2,2,64,256]{3,2,1,0:T(8,128)(2,1)}, u32[]{:S(2)}, u32[]{:S(2)}) collective-permute-start(bf16[2,2,64,256]{3,2,1,0:T(8,128)(2,1)} %slice.36), channel_id=1, source_target_pairs={{0,8},{8,16},{16,24},{24,0},{1,9},{9,17},{17,25},{25,1},{2,10},{10... | collective-permute-start | bytes 393224 | tf_op jit(solution)/shard_map/ppermute | solution.py:263
  111.6 12.3 %collective-permute-start.8 = (bf16[4,64,2048]{2,1,0:T(8,128)(2,1)S(1)}, bf16[4,64,2048]{2,1,0:T(8,128)(2,1)S(1)}, u32[]{:S(2)}, u32[]{:S(2)}) collective-permute-start(bf16[4,64,2048]{2,1,0:T(8,128)(2,1)S(1)} %project.3), channel_id=1, source_target_pairs={{0,1},{1,0},{2,3},{3,2},{4,5},{5,4},{6,7},{7,6},{8,9},{9,8},{10,11... | collective-permute-start | bytes 3145736 | tf_op jit(solution)/shard_map/ppermute | solution.py:259
  125.3 18.7 %copy-start.8 = (f32[2048]{0:T(1024)S(1)}, f32[2048]{0:T(1024)}, u32[]{:S(2)}) copy-start(f32[2048]{0:T(1024)} %param.23) | copy-start | bytes 24580
  125.3 18.7 %all-to-all-start.2 = ((bf16[4,64,2048]{2,1,0:T(8,128)(2,1)}), bf16[4,64,2048]{2,1,0:T(8,128)(2,1)S(1)}, u32[]{:S(2)}, u32[]{:S(2)}) async-start(bf16[4,64,2048]{2,1,0:T(8,128)(2,1)} %add_convert_fusion.1), calls=%async_computation.2 | async-start | bytes 2097152 | tf_op jit(solution)/shard_map/all_to_all | solution.py:275
  160.4 8.5 %collective-permute-start.12 = (bf16[4,64,2048]{2,1,0:T(8,128)(2,1)S(1)}, bf16[4,64,2048]{2,1,0:T(8,128)(2,1)S(1)}, u32[]{:S(2)}, u32[]{:S(2)}) collective-permute-start(bf16[4,64,2048]{2,1,0:T(8,128)(2,1)S(1)} %all_to_all.27.rows_hbm), channel_id=1, source_target_pairs={{0,1},{1,0},{2,3},{3,2},{4,5},{5,4},{6,7},{7,6},{8,9},{9,8},{10,11... | collective-permute-start | bytes 3145736 | tf_op jit(solution)/shard_map/ppermute | solution.py:259
  171.5 4.6 %collective-permute-start.13 = (bf16[4,64,2048]{2,1,0:T(8,128)(2,1)S(1)}, bf16[4,64,2048]{2,1,0:T(8,128)(2,1)S(1)}, u32[]{:S(2)}, u32[]{:S(2)}) collective-permute-start(bf16[4,64,2048]{2,1,0:T(8,128)(2,1)S(1)} %feed.3), channel_id=1, source_target_pairs={{0,1},{1,0},{2,3},{3,2},{4,5},{5,4},{6,7},{7,6},{8,9},{9,8},{10,11... | collective-permute-start | bytes 3145736 | tf_op jit(solution)/shard_map/ppermute | solution.py:259
  176.2 17.5 %copy-start.9 = (f32[2048]{0:T(1024)S(1)}, f32[2048]{0:T(1024)}, u32[]{:S(2)}) copy-start(f32[2048]{0:T(1024)} %param.27) | copy-start | bytes 24580
  (7 other events, 11.1 us)
Sparse Core Ops, SparseCore 0:
  25.4 116.8 all-gather.2

commit v3 on v2

--- a/solution.py
+++ b/solution.py
@@ -74,7 +74,7 @@
     param = decay_ref[...]
     softplus = jnp.maximum(-param, 0.0) + jnp.log1p(jnp.exp(-jnp.abs(param)))
     late.wait()
-    log_a = rate * (-8.0 * softplus) + shift_ref[...]
+    log_a = -8.0 * rate * softplus + shift_ref[...]
     a = jnp.exp(log_a)
     drive = jnp.sqrt(-jnp.tanh(log_a) * (1.0 + a * a)) * inlet * conv.astype(f32)
     tiles = length // 8
@@ -320,7 +320,9 @@
     first = jnp.concatenate(
         [recurrence_branch_weight, gate_branch_weight, recurrence_output_weight.T], axis=1
     )
-    pair = copy_for_each(first, "zh")
+    across = lax.ppermute(first, "zh", [(0, 1), (1, 0)])
+    low = lax.axis_index("zh") == 0
+    pair = jnp.stack([jnp.where(low, first, across), jnp.where(low, across, first)])
     line = copy_for_each(pair, "zl")
     branch_weight = round_y(line[..., : 2 * channels])
     output_weight = round_y(line[..., 2 * channels :])

time: 204 us -> 204 us (level)
  blocking collectives: 78.7 us -> 72 us
  starting transfers between devices: 54.8 us -> 58.7 us
  waiting for transfers between devices: 21.5 us -> 24.8 us
    ppermute x0 -> x1, starting transfers between devices: none -> 7.87 us  [local(): across = lax.ppermute(first, 'zh', [(0, 1), (1, 0)])]
    all_to_all x2 -> x1, blocking collectives: 45.7 us -> 39.1 us  [copy_for_each(): return lax.all_to_all(copies, axis, split_axis=0, concat_axis=0, tiled=True)]
    ppermute x3, starting transfers between devices: 16.5 us -> 13.6 us  [to_partner(): return lax.ppermute(value, 'c', [(0, 1), (1, 0)])]
  transfers between devices with their start and end apart: 16 -> 17, of which waited for: 4 -> 5; matrix products, arithmetic and copies ran while one was open for 2% -> 2% of each run, Pallas kernels for 8% -> 8%
where the time goes in v3:
time: 204 us; the launch traced here: 202 us
  blocking collectives  72 us (35%)
  starting transfers between devices  58.7 us (29%)
  waiting for transfers between devices  24.8 us (12%)
  Pallas kernels  20.1 us (10%)
  between operations  13.9 us (7%)
  local copies, waits for them, and re-layouts  8.17 us (4%)
  other arithmetic  4.62 us (2%)
    all_to_all x1, blocking collectives, copy_for_each(): return lax.all_to_all(copies, axis, split_axis=0, concat_axis=0, tiled=True)  39.1 us
    ppermute x11, starting transfers between devices, sideways(): return lax.ppermute(value, 'y', [(i, (i + by) % 4) for i in range(4)])  33.2 us
    all_to_all x1, blocking collectives, sum_at_owner(): return lax.all_to_all(both, 'x', 0, 0, tiled=True)  17.1 us
    all_to_all x1, blocking collectives, local(): mine = lax.all_to_all(copies, 'x', 0, 0, tiled=True)  15.8 us
    all_to_all x1, waiting for transfers between devices, sum_at_owner(): return lax.all_to_all(both, 'x', 0, 0, tiled=True)  14.5 us
    ppermute x3, starting transfers between devices, to_partner(): return lax.ppermute(value, 'c', [(0, 1), (1, 0)])  13.6 us
    ppermute x11, waiting for transfers between devices, sideways(): return lax.ppermute(value, 'y', [(i, (i + by) % 4) for i in range(4)])  8.24 us
    ppermute x1, starting transfers between devices, local(): across = lax.ppermute(first, 'zh', [(0, 1), (1, 0)])  7.87 us
  transfers between devices with their start and end apart: 17, of which 5 were waited for; matrix products, arithmetic and copies ran while one was open for 2% of the time, Pallas kernels for 8%

profile of v3, /device:TPU:1, one launch (start us, length us, event | category | flops | bytes accessed | tf_op | source)
XLA Modules:
  0.0 202.4 jit_solution(6530098911963602008)
XLA Ops:
  8.3 5.6 %collective-permute-start.12 = (bf16[96,640]{1,0:T(8,128)(2,1)S(1)}, bf16[96,640]{1,0:T(8,128)(2,1)S(1)}, u32[]{:S(2)}, u32[]{:S(2)}) collective-permute-start(bf16[96,640]{1,0:T(8,128)(2,1)S(1)} %pad_maximum_fusion.2), channel_id=1, source_target_pairs={{0,16},{8,24},{16,0},{24,8},{1,17},{9,25},{17,1},{25,9},{2,18},{10... | collective-permute-start | bytes 368648 | tf_op jit(solution)/shard_map/ppermute | solution.py:263
  13.9 2.7 %collective-permute-start.11 = (bf16[96,640]{1,0:T(8,128)(2,1)S(1)}, bf16[96,640]{1,0:T(8,128)(2,1)S(1)}, u32[]{:S(2)}, u32[]{:S(2)}) collective-permute-start(bf16[96,640]{1,0:T(8,128)(2,1)S(1)} %pad_maximum_fusion.2), channel_id=1, source_target_pairs={{0,24},{8,0},{16,8},{24,16},{1,25},{9,1},{17,9},{25,17},{2,26},{10... | collective-permute-start | bytes 368648 | tf_op jit(solution)/shard_map/ppermute | solution.py:263
  16.6 2.6 %collective-permute-start.10 = (bf16[96,640]{1,0:T(8,128)(2,1)S(1)}, bf16[96,640]{1,0:T(8,128)(2,1)S(1)}, u32[]{:S(2)}, u32[]{:S(2)}) collective-permute-start(bf16[96,640]{1,0:T(8,128)(2,1)S(1)} %pad_maximum_fusion.2), channel_id=1, source_target_pairs={{0,8},{8,16},{16,24},{24,0},{1,9},{9,17},{17,25},{25,1},{2,10},{10... | collective-permute-start | bytes 368648 | tf_op jit(solution)/shard_map/ppermute | solution.py:263
  19.6 4.8 %collective-permute-done.10 = bf16[96,640]{1,0:T(8,128)(2,1)S(1)} collective-permute-done((bf16[96,640]{1,0:T(8,128)(2,1)S(1)}, bf16[96,640]{1,0:T(8,128)(2,1)S(1)}, u32[]{:S(2)}, u32[]{:S(2)}) %collective-permute-start.10) | collective-permute-done | bytes 122912 | tf_op jit(solution)/shard_map/ppermute | solution.py:263
  25.3 7.9 %collective-permute-start = (bf16[64,768]{1,0:T(8,128)(2,1)S(1)}, bf16[64,768]{1,0:T(8,128)(2,1)S(1)}, u32[]{:S(2)}, u32[]{:S(2)}) collective-permute-start(bf16[64,768]{1,0:T(8,128)(2,1)S(1)} %pad_maximum_fusion.3), channel_id=1, source_target_pairs={{0,128},{128,0},{1,129},{129,1},{2,130},{130,2},{3,131},{131,3},{4... | collective-permute-start | bytes 294920 | tf_op jit(solution)/shard_map/ppermute | solution.py:323
  35.4 39.1 %all_to_all.20 = bf16[4,2,64,768]{3,2,1,0:T(8,128)(2,1)S(1)} all-to-all(bf16[4,2,64,768]{3,2,1,0:T(8,128)(2,1)S(1)} %broadcast_in_dim.3), channel_id=1, replica_groups=mesh['r'=2,'zh'=2,'zl'=4,'y'=4,'x'=4,'c'=2] {'zl'}, dimensions={0} | all-to-all | bytes 1572864 | tf_op jit(solution)/shard_map/all_to_all | solution.py:21
  76.4 3.4 %collective-permute-start.1 = (bf16[4,2,64,512]{3,2,1,0:T(8,128)(2,1)S(1)}, bf16[4,2,64,512]{3,2,1,0:T(8,128)(2,1)S(1)}, u32[]{:S(2)}, u32[]{:S(2)}) collective-permute-start(bf16[4,2,64,512]{3,2,1,0:T(8,128)(2,1)S(1)} %slice.32.refs_0_), channel_id=1, source_target_pairs={{0,8},{8,16},{16,24},{24,0},{1,9},{9,17},{17,25},{25,1},{2,10},{10... | collective-permute-start | bytes 1572872 | tf_op jit(solution)/shard_map/ppermute | solution.py:263
  79.8 3.1 %collective-permute-start.6 = (bf16[4,2,64,256]{3,2,1,0:T(8,128)(2,1)S(1)}, bf16[4,2,64,256]{3,2,1,0:T(8,128)(2,1)S(1)}, u32[]{:S(2)}, u32[]{:S(2)}) collective-permute-start(bf16[4,2,64,256]{3,2,1,0:T(8,128)(2,1)S(1)} %slice.35.refs_0_), channel_id=1, source_target_pairs={{0,24},{8,0},{16,8},{24,16},{1,25},{9,1},{17,9},{25,17},{2,26},{10... | collective-permute-start | bytes 786440 | tf_op jit(solution)/shard_map/ppermute | solution.py:263
  83.0 2.2 %collective-permute-start.5 = (bf16[4,2,64,256]{3,2,1,0:T(8,128)(2,1)S(1)}, bf16[4,2,64,256]{3,2,1,0:T(8,128)(2,1)S(1)}, u32[]{:S(2)}, u32[]{:S(2)}) collective-permute-start(bf16[4,2,64,256]{3,2,1,0:T(8,128)(2,1)S(1)} %slice.35.refs_0_), channel_id=1, source_target_pairs={{0,8},{8,16},{16,24},{24,0},{1,9},{9,17},{17,25},{25,1},{2,10},{10... | collective-permute-start | bytes 786440 | tf_op jit(solution)/shard_map/ppermute | solution.py:263
  85.1 3.1 %collective-permute-done.2.refs_2_ = bf16[4,2,64,512]{3,2,1,0:T(8,128)(2,1)S(1)} collective-permute-done((bf16[4,2,64,512]{3,2,1,0:T(8,128)(2,1)S(1)}, bf16[4,2,64,512]{3,2,1,0:T(8,128)(2,1)S(1)}, u32[]{:S(2)}, u32[]{:S(2)}) %collective-permute-start.2) | collective-permute-done | bytes 524320 | tf_op jit(solution)/shard_map/ppermute | solution.py:263
  89.0 3.3 %collective-permute-start.4 = (bf16[2,2,64,512]{3,2,1,0:T(8,128)(2,1)}, bf16[2,2,64,512]{3,2,1,0:T(8,128)(2,1)}, u32[]{:S(2)}, u32[]{:S(2)}) collective-permute-start(bf16[2,2,64,512]{3,2,1,0:T(8,128)(2,1)} %slice.34), channel_id=1, source_target_pairs={{0,24},{8,0},{16,8},{24,16},{1,25},{9,1},{17,9},{25,17},{2,26},{10... | collective-permute-start | bytes 786440 | tf_op jit(solution)/shard_map/ppermute | solution.py:263
  95.9 4.5 %collective-permute-start.8 = (bf16[2,2,64,256]{3,2,1,0:T(8,128)(2,1)}, bf16[2,2,64,256]{3,2,1,0:T(8,128)(2,1)S(1)}, u32[]{:S(2)}, u32[]{:S(2)}) collective-permute-start(bf16[2,2,64,256]{3,2,1,0:T(8,128)(2,1)} %slice.37), channel_id=1, source_target_pairs={{0,24},{8,0},{16,8},{24,16},{1,25},{9,1},{17,9},{25,17},{2,26},{10... | collective-permute-start | bytes 393224 | tf_op jit(solution)/shard_map/ppermute | solution.py:263
  108.2 4.7 %mix.1.branch_hbm = bf16[512,256]{1,0:T(8,128)(2,1)S(1)} custom-call(s32[2]{0:T(128)S(1)} %pad_add_fusion.place_ref, bf16[512,2048]{1,0:T(8,128)(2,1)S(1)} %copy-done, bf16[4,2,64,512]{3,2,1,0:T(8,128)(2,1)S(1)} %slice.32.refs_0_, bf16[4,2,64,512]{3,2,1,0:T(8,128)(2,1)S(1)} %copy-done.4, bf16[4,2,64,512]{3,2,1,0:T(8,128)(2,1)S(1)} %copy-done.2, ...), custom_call_target="tpu_custom_call" | custom-call | tf_op jit(solution)/shard_map/mix/pallas_call | solution.py:103
  112.8 2.3 %project.3 = bf16[4,64,2048]{2,1,0:T(8,128)(2,1)S(1)} custom-call(s32[2]{0:T(128)S(1)} %pad_add_fusion.1.place_ref, bf16[512,256]{1,0:T(8,128)(2,1)S(1)} %mix.1.branch_hbm, bf16[4,2,64,256]{3,2,1,0:T(8,128)(2,1)S(1)} %slice.35.refs_0_, bf16[4,2,64,256]{3,2,1,0:T(8,128)(2,1)S(1)} %collective-permute-done.5.refs_1_, ...), custom_call_target="tpu_custom_call" | custom-call | tf_op jit(solution)/shard_map/project/pallas_call | solution.py:148
  115.1 7.1 %collective-permute-start.9 = (bf16[4,64,2048]{2,1,0:T(8,128)(2,1)S(1)}, bf16[4,64,2048]{2,1,0:T(8,128)(2,1)S(1)}, u32[]{:S(2)}, u32[]{:S(2)}) collective-permute-start(bf16[4,64,2048]{2,1,0:T(8,128)(2,1)S(1)} %project.3), channel_id=1, source_target_pairs={{0,1},{1,0},{2,3},{3,2},{4,5},{5,4},{6,7},{7,6},{8,9},{9,8},{10,11... | collective-permute-start | bytes 3145736 | tf_op jit(solution)/shard_map/ppermute | solution.py:259
  122.2 2.3 %project.2 = bf16[4,64,2048]{2,1,0:T(8,128)(2,1)S(1)} custom-call(s32[2]{0:T(128)S(1)} %pad_add_fusion.place_ref, bf16[512,256]{1,0:T(8,128)(2,1)S(1)} %mix.1.branch_hbm, bf16[4,2,64,256]{3,2,1,0:T(8,128)(2,1)S(1)} %slice.35.refs_0_, bf16[4,2,64,256]{3,2,1,0:T(8,128)(2,1)S(1)} %collective-permute-done.5.refs_1_, ...), custom_call_target="tpu_custom_call" | custom-call | tf_op jit(solution)/shard_map/project/pallas_call | solution.py:148
  125.9 4.1 %all-to-all-start.1 = ((bf16[4,64,2048]{2,1,0:T(8,128)(2,1)}), bf16[4,64,2048]{2,1,0:T(8,128)(2,1)S(1)}, u32[]{:S(2)}, u32[]{:S(2)}) async-start(bf16[4,64,2048]{2,1,0:T(8,128)(2,1)} %add_convert_fusion.1), calls=%async_computation.1 | async-start | bytes 2097152 | tf_op jit(solution)/shard_map/all_to_all | solution.py:275
  130.1 14.5 %all-to-all-done.1.parts_hbm = bf16[4,64,2048]{2,1,0:T(8,128)(2,1)S(1)} async-done(((bf16[4,64,2048]{2,1,0:T(8,128)(2,1)}), bf16[4,64,2048]{2,1,0:T(8,128)(2,1)S(1)}, u32[]{:S(2)}, u32[]{:S(2)}) %all-to-all-start.1) | async-done | bytes 1048608 | tf_op jit(solution)/shard_map/all_to_all | solution.py:275
  145.2 15.8 %all_to_all.21.rows_hbm = bf16[4,64,2048]{2,1,0:T(8,128)(2,1)S(1)} all-to-all(bf16[4,64,2048]{2,1,0:T(8,128)(2,1)S(1)} %get-tuple-element.10), channel_id=1, replica_groups=mesh['r'=2,'zh'=2,'zl'=4,'y'=4,'x'=4,'c'=2] {'x'}, dimensions={0} | all-to-all | bytes 2097152 | tf_op jit(solution)/shard_map/all_to_all | solution.py:343
  161.0 4.5 %collective-permute-start.13 = (bf16[4,64,2048]{2,1,0:T(8,128)(2,1)S(1)}, bf16[4,64,2048]{2,1,0:T(8,128)(2,1)S(1)}, u32[]{:S(2)}, u32[]{:S(2)}) collective-permute-start(bf16[4,64,2048]{2,1,0:T(8,128)(2,1)S(1)} %all_to_all.21.rows_hbm), channel_id=1, source_target_pairs={{0,1},{1,0},{2,3},{3,2},{4,5},{5,4},{6,7},{7,6},{8,9},{9,8},{10,11... | collective-permute-start | bytes 3145736 | tf_op jit(solution)/shard_map/ppermute | solution.py:259
  165.6 3.9 %stage.1 = (bf16[8,4,64,640]{3,2,1,0:T(8,128)(2,1)S(1)}, bf16[8,4,64,640]{3,2,1,0:T(8,128)(2,1)S(1)}, bf16[8,4,2,32,640]{4,3,2,1,0:T(8,128)(2,1)S(1)}) custom-call(s32[2]{0:T(128)S(1)} %pad_add_fusion.place_ref, bf16[2,8,4,96,640]{4,3,2,1,0:T(8,128)(2,1)} %bitcast.24), custom_call_target="tpu_custom_call" | custom-call | tf_op jit(solution)/shard_map/stage/pallas_call | solution.py:222
  169.5 2.7 %feed.3 = bf16[4,64,2048]{2,1,0:T(8,128)(2,1)S(1)} custom-call(bf16[4,64,2048]{2,1,0:T(8,128)(2,1)S(1)} %collective-permute-done.13.rows_hbm, bf16[8,4,64,640]{3,2,1,0:T(8,128)(2,1)S(1)} %get-tuple-element.11.gate_ref, bf16[8,4,64,640]{3,2,1,0:T(8,128)(2,1)S(1)} %get-tuple-element.12.up_ref, bf16[8,4,2,32,640]{4,3,2,1,0:T(8,128)(2,1)S(1)} %get-tuple-element.13.down_ref), custom_call_target="tpu_custom_call" | custom-call | tf_op jit(solution)/shard_map/feed/pallas_call | solution.py:247
  174.1 2.7 %feed.2 = bf16[4,64,2048]{2,1,0:T(8,128)(2,1)S(1)} custom-call(bf16[4,64,2048]{2,1,0:T(8,128)(2,1)S(1)} %all_to_all.21.rows_hbm, bf16[8,4,64,640]{3,2,1,0:T(8,128)(2,1)S(1)} %get-tuple-element.11.gate_ref, bf16[8,4,64,640]{3,2,1,0:T(8,128)(2,1)S(1)} %get-tuple-element.12.up_ref, bf16[8,4,2,32,640]{4,3,2,1,0:T(8,128)(2,1)S(1)} %get-tuple-element.13.down_ref), custom_call_target="tpu_custom_call" | custom-call | tf_op jit(solution)/shard_map/feed/pallas_call | solution.py:247
  177.2 17.1 %all_to_all.22.parts_hbm = bf16[4,64,2048]{2,1,0:T(8,128)(2,1)S(1)} all-to-all(bf16[4,64,2048]{2,1,0:T(8,128)(2,1)S(1)} %add_convert_fusion), channel_id=1, replica_groups=mesh['r'=2,'zh'=2,'zl'=4,'y'=4,'x'=4,'c'=2] {'x'}, dimensions={0} | all-to-all | bytes 2097152 | tf_op jit(solution)/shard_map/all_to_all | solution.py:275
  (71 shorter events, 24.5 us)
Async XLA Ops:
  6.5 18.8 %copy-start.13 = (bf16[64,256]{1,0:T(8,128)(2,1)S(1)}, bf16[64,256]{1,0:T(8,128)(2,1)}, u32[]{:S(2)}) copy-start(bf16[64,256]{1,0:T(8,128)(2,1)} %param.16) | copy-start | bytes 98308
  6.5 18.8 %copy-start.14 = (bf16[64,256]{1,0:T(8,128)(2,1)S(1)}, bf16[64,256]{1,0:T(8,128)(2,1)}, u32[]{:S(2)}) copy-start(bf16[64,256]{1,0:T(8,128)(2,1)} %param.15) | copy-start | bytes 98308
  6.5 18.8 %copy-start.12 = (bf16[256,64]{0,1:T(8,128)(2,1)S(1)}, bf16[256,64]{0,1:T(8,128)(2,1)}, u32[]{:S(2)}) copy-start(bf16[256,64]{0,1:T(8,128)(2,1)} %param.22) | copy-start | bytes 98308
  6.5 159.0 %all-gather.3.cloned.1.call-start = ((), (), s32[]{:S(2)}) async-start(), calls=%async_computation.4 | async-start | bytes 8355840 | tf_op jit(solution)/shard_map/all_gather | solution.py:317
  8.3 10.9 %collective-permute-start.12 = (bf16[96,640]{1,0:T(8,128)(2,1)S(1)}, bf16[96,640]{1,0:T(8,128)(2,1)S(1)}, u32[]{:S(2)}, u32[]{:S(2)}) collective-permute-start(bf16[96,640]{1,0:T(8,128)(2,1)S(1)} %pad_maximum_fusion.2), channel_id=1, source_target_pairs={{0,16},{8,24},{16,0},{24,8},{1,17},{9,25},{17,1},{25,9},{2,18},{10... | collective-permute-start | bytes 368648 | tf_op jit(solution)/shard_map/ppermute | solution.py:263
  13.9 5.6 %collective-permute-start.11 = (bf16[96,640]{1,0:T(8,128)(2,1)S(1)}, bf16[96,640]{1,0:T(8,128)(2,1)S(1)}, u32[]{:S(2)}, u32[]{:S(2)}) collective-permute-start(bf16[96,640]{1,0:T(8,128)(2,1)S(1)} %pad_maximum_fusion.2), channel_id=1, source_target_pairs={{0,24},{8,0},{16,8},{24,16},{1,25},{9,1},{17,9},{25,17},{2,26},{10... | collective-permute-start | bytes 368648 | tf_op jit(solution)/shard_map/ppermute | solution.py:263
  16.6 7.8 %collective-permute-start.10 = (bf16[96,640]{1,0:T(8,128)(2,1)S(1)}, bf16[96,640]{1,0:T(8,128)(2,1)S(1)}, u32[]{:S(2)}, u32[]{:S(2)}) collective-permute-start(bf16[96,640]{1,0:T(8,128)(2,1)S(1)} %pad_maximum_fusion.2), channel_id=1, source_target_pairs={{0,8},{8,16},{16,24},{24,0},{1,9},{9,17},{17,25},{25,1},{2,10},{10... | collective-permute-start | bytes 368648 | tf_op jit(solution)/shard_map/ppermute | solution.py:263
  25.3 9.9 %collective-permute-start = (bf16[64,768]{1,0:T(8,128)(2,1)S(1)}, bf16[64,768]{1,0:T(8,128)(2,1)S(1)}, u32[]{:S(2)}, u32[]{:S(2)}) collective-permute-start(bf16[64,768]{1,0:T(8,128)(2,1)S(1)} %pad_maximum_fusion.3), channel_id=1, source_target_pairs={{0,128},{128,0},{1,129},{129,1},{2,130},{130,2},{3,131},{131,3},{4... | collective-permute-start | bytes 294920 | tf_op jit(solution)/shard_map/ppermute | solution.py:323
  35.3 67.9 %copy-start = (bf16[512,2048]{1,0:T(8,128)(2,1)S(1)}, bf16[512,2048]{1,0:T(8,128)(2,1)}, u32[]{:S(2)}) copy-start(bf16[512,2048]{1,0:T(8,128)(2,1)} %tokens_hbm.1) | copy-start | bytes 6291460
  35.3 67.8 %copy-start.10 = (bf16[4,256]{1,0:T(4,128)(2,1)S(1)}, bf16[4,256]{1,0:T(4,128)(2,1)}, u32[]{:S(2)}) copy-start(bf16[4,256]{1,0:T(4,128)(2,1)} %refs_5_.1) | copy-start | bytes 6148
  35.4 67.8 %copy-start.11 = (f32[256]{0:T(256)S(1)}, f32[256]{0:T(256)}, u32[]{:S(2)}) copy-start(f32[256]{0:T(256)} %param.20) | copy-start | bytes 3076
  74.5 13.7 %collective-permute-start.2 = (bf16[4,2,64,512]{3,2,1,0:T(8,128)(2,1)S(1)}, bf16[4,2,64,512]{3,2,1,0:T(8,128)(2,1)S(1)}, u32[]{:S(2)}, u32[]{:S(2)}) collective-permute-start(bf16[4,2,64,512]{3,2,1,0:T(8,128)(2,1)S(1)} %slice.32.refs_0_), channel_id=1, source_target_pairs={{0,24},{8,0},{16,8},{24,16},{1,25},{9,1},{17,9},{25,17},{2,26},{10... | collective-permute-start | bytes 1572872 | tf_op jit(solution)/shard_map/ppermute | solution.py:263
  76.4 15.8 %collective-permute-start.1 = (bf16[4,2,64,512]{3,2,1,0:T(8,128)(2,1)S(1)}, bf16[4,2,64,512]{3,2,1,0:T(8,128)(2,1)S(1)}, u32[]{:S(2)}, u32[]{:S(2)}) collective-permute-start(bf16[4,2,64,512]{3,2,1,0:T(8,128)(2,1)S(1)} %slice.32.refs_0_), channel_id=1, source_target_pairs={{0,8},{8,16},{16,24},{24,0},{1,9},{9,17},{17,25},{25,1},{2,10},{10... | collective-permute-start | bytes 1572872 | tf_op jit(solution)/shard_map/ppermute | solution.py:263
  79.8 15.4 %collective-permute-start.6 = (bf16[4,2,64,256]{3,2,1,0:T(8,128)(2,1)S(1)}, bf16[4,2,64,256]{3,2,1,0:T(8,128)(2,1)S(1)}, u32[]{:S(2)}, u32[]{:S(2)}) collective-permute-start(bf16[4,2,64,256]{3,2,1,0:T(8,128)(2,1)S(1)} %slice.35.refs_0_), channel_id=1, source_target_pairs={{0,24},{8,0},{16,8},{24,16},{1,25},{9,1},{17,9},{25,17},{2,26},{10... | collective-permute-start | bytes 786440 | tf_op jit(solution)/shard_map/ppermute | solution.py:263
  83.0 17.5 %collective-permute-start.5 = (bf16[4,2,64,256]{3,2,1,0:T(8,128)(2,1)S(1)}, bf16[4,2,64,256]{3,2,1,0:T(8,128)(2,1)S(1)}, u32[]{:S(2)}, u32[]{:S(2)}) collective-permute-start(bf16[4,2,64,256]{3,2,1,0:T(8,128)(2,1)S(1)} %slice.35.refs_0_), channel_id=1, source_target_pairs={{0,8},{8,16},{16,24},{24,0},{1,9},{9,17},{17,25},{25,1},{2,10},{10... | collective-permute-start | bytes 786440 | tf_op jit(solution)/shard_map/ppermute | solution.py:263
  89.0 14.2 %collective-permute-start.4 = (bf16[2,2,64,512]{3,2,1,0:T(8,128)(2,1)}, bf16[2,2,64,512]{3,2,1,0:T(8,128)(2,1)}, u32[]{:S(2)}, u32[]{:S(2)}) collective-permute-start(bf16[2,2,64,512]{3,2,1,0:T(8,128)(2,1)} %slice.34), channel_id=1, source_target_pairs={{0,24},{8,0},{16,8},{24,16},{1,25},{9,1},{17,9},{25,17},{2,26},{10... | collective-permute-start | bytes 786440 | tf_op jit(solution)/shard_map/ppermute | solution.py:263
  93.3 9.9 %collective-permute-start.3 = (bf16[2,2,64,512]{3,2,1,0:T(8,128)(2,1)}, bf16[2,2,64,512]{3,2,1,0:T(8,128)(2,1)}, u32[]{:S(2)}, u32[]{:S(2)}) collective-permute-start(bf16[2,2,64,512]{3,2,1,0:T(8,128)(2,1)} %slice.33), channel_id=1, source_target_pairs={{0,8},{8,16},{16,24},{24,0},{1,9},{9,17},{17,25},{25,1},{2,10},{10... | collective-permute-start | bytes 786440 | tf_op jit(solution)/shard_map/ppermute | solution.py:263
  95.9 16.9 %collective-permute-start.8 = (bf16[2,2,64,256]{3,2,1,0:T(8,128)(2,1)}, bf16[2,2,64,256]{3,2,1,0:T(8,128)(2,1)S(1)}, u32[]{:S(2)}, u32[]{:S(2)}) collective-permute-start(bf16[2,2,64,256]{3,2,1,0:T(8,128)(2,1)} %slice.37), channel_id=1, source_target_pairs={{0,24},{8,0},{16,8},{24,16},{1,25},{9,1},{17,9},{25,17},{2,26},{10... | collective-permute-start | bytes 393224 | tf_op jit(solution)/shard_map/ppermute | solution.py:263
  101.1 11.7 %collective-permute-start.7 = (bf16[2,2,64,256]{3,2,1,0:T(8,128)(2,1)}, bf16[2,2,64,256]{3,2,1,0:T(8,128)(2,1)}, u32[]{:S(2)}, u32[]{:S(2)}) collective-permute-start(bf16[2,2,64,256]{3,2,1,0:T(8,128)(2,1)} %slice.36), channel_id=1, source_target_pairs={{0,8},{8,16},{16,24},{24,0},{1,9},{9,17},{17,25},{25,1},{2,10},{10... | collective-permute-start | bytes 393224 | tf_op jit(solution)/shard_map/ppermute | solution.py:263
  115.1 9.4 %collective-permute-start.9 = (bf16[4,64,2048]{2,1,0:T(8,128)(2,1)S(1)}, bf16[4,64,2048]{2,1,0:T(8,128)(2,1)S(1)}, u32[]{:S(2)}, u32[]{:S(2)}) collective-permute-start(bf16[4,64,2048]{2,1,0:T(8,128)(2,1)S(1)} %project.3), channel_id=1, source_target_pairs={{0,1},{1,0},{2,3},{3,2},{4,5},{5,4},{6,7},{7,6},{8,9},{9,8},{10,11... | collective-permute-start | bytes 3145736 | tf_op jit(solution)/shard_map/ppermute | solution.py:259
  125.9 18.7 %copy-start.8 = (f32[2048]{0:T(1024)S(1)}, f32[2048]{0:T(1024)}, u32[]{:S(2)}) copy-start(f32[2048]{0:T(1024)} %param.23) | copy-start | bytes 24580
  125.9 18.7 %all-to-all-start.1 = ((bf16[4,64,2048]{2,1,0:T(8,128)(2,1)}), bf16[4,64,2048]{2,1,0:T(8,128)(2,1)S(1)}, u32[]{:S(2)}, u32[]{:S(2)}) async-start(bf16[4,64,2048]{2,1,0:T(8,128)(2,1)} %add_convert_fusion.1), calls=%async_computation.1 | async-start | bytes 2097152 | tf_op jit(solution)/shard_map/all_to_all | solution.py:275
  161.0 8.5 %collective-permute-start.13 = (bf16[4,64,2048]{2,1,0:T(8,128)(2,1)S(1)}, bf16[4,64,2048]{2,1,0:T(8,128)(2,1)S(1)}, u32[]{:S(2)}, u32[]{:S(2)}) collective-permute-start(bf16[4,64,2048]{2,1,0:T(8,128)(2,1)S(1)} %all_to_all.21.rows_hbm), channel_id=1, source_target_pairs={{0,1},{1,0},{2,3},{3,2},{4,5},{5,4},{6,7},{7,6},{8,9},{9,8},{10,11... | collective-permute-start | bytes 3145736 | tf_op jit(solution)/shard_map/ppermute | solution.py:259
  172.2 4.6 %collective-permute-start.14 = (bf16[4,64,2048]{2,1,0:T(8,128)(2,1)S(1)}, bf16[4,64,2048]{2,1,0:T(8,128)(2,1)S(1)}, u32[]{:S(2)}, u32[]{:S(2)}) collective-permute-start(bf16[4,64,2048]{2,1,0:T(8,128)(2,1)S(1)} %feed.3), channel_id=1, source_target_pairs={{0,1},{1,0},{2,3},{3,2},{4,5},{5,4},{6,7},{7,6},{8,9},{9,8},{10,11... | collective-permute-start | bytes 3145736 | tf_op jit(solution)/shard_map/ppermute | solution.py:259
  (8 other events, 27.5 us)
Sparse Core Ops, SparseCore 0:
  25.4 116.8 all-gather.2
